TPU v7x, 256 devices: a whole 4x4x8 slice. The times are simulated.
256 devices in a mesh: sp: 16 (over y, x), tp: 16 (over z, core).
Axes of the slice: x: 4, y: 4, z: 8, core: 2. Of those that a mesh axis runs over, the one named last changes fastest.
Arguments:
- layer_in: bfloat16 [5120, 2048], P('sp', 'tp'), may hold values from -6 to 6
- out_cot: bfloat16 [5120, 2048], P('sp', 'tp'), may hold values from -6 to 6
- route_ids: int32 [5120, 2], P('sp'), may hold values from 0 to 15, all different within a row; in each aligned block of 320 rows (0 to 319, 320 to 639, ...) at most 80 rows name the same one
- route_probs: float32 [5120, 2], P('sp'), may hold values from 0.2 to 1
- group_prob: float32 [5120], P('sp'), may hold values from 0.3 to 1
- gate_weight: bfloat16 [16, 2048, 2048], P('sp', 'tp'), may hold values from -0.125 to 0.125
- up_weight: bfloat16 [16, 2048, 2048], P('sp', 'tp'), may hold values from -0.125 to 0.125
- down_weight: bfloat16 [16, 2048, 2048], P('sp', 'tp'), may hold values from -0.125 to 0.125
- out_weight: bfloat16 [2048, 2048], P(None, 'tp'), may hold values from -0.125 to 0.125
- query: bfloat16 [5120, 1024], P('sp', 'tp'), may hold values from -6 to 6
- key_in: bfloat16 [5120, 1024], P('sp', 'tp'), may hold values from -0.75 to 0.75
- value: bfloat16 [5120, 2048], P('sp', 'tp'), may hold values from -6 to 6
- decay_logit: bfloat16 [5120, 1024], P('sp', 'tp'), may hold values from -2.5 to 8.5, as said below
Outputs:
- gate_grad: float32 [16, 2048, 2048], P('sp', 'tp')
- up_grad: float32 [16, 2048, 2048], P('sp', 'tp')
- down_grad: float32 [16, 2048, 2048], P('sp', 'tp')
- proj_grad: float32 [2048, 2048], P('sp', 'tp')
- query_grad: float32 [5120, 1024], P('sp', 'tp')
- key_grad: float32 [5120, 1024], P('sp', 'tp')
- value_grad: float32 [5120, 2048], P('sp', 'tp')
- logit_grad: float32 [5120, 1024], P('sp', 'tp')
Inputs may be any that keep to these rules, and one draw needn't show every extreme that they name: `route_ids`: each row names two different experts of 0 to 15; every expert is named by some row; within each aligned block of 320 rows (the rows of one device) no expert is named more than 80 times, and in some block one expert is named exactly 80 times. `decay_logit`: values lie between -2.5 and 8.5; even heads have pre-activations near 5, odd heads near 1.
All inputs are finite; a program needn't handle non-finite values.
Results may differ from a plain program's by a relative error of at most 0.019.
Values may be sent and summed in bfloat16 or wider, within the bound.
A program may use at most 128 MiB of HBM per device.

v0:
```python
import jax
import jax.numpy as jnp
from jax import lax
from jax.sharding import PartitionSpec as P

DK = 64
DV = 128
BLOCK = 64


decay_temp = 16.0
highest = lax.Precision.HIGHEST


def side_by_side(arrays, axis, dim, along):
    both = jnp.concatenate(arrays, axis=along)
    filled, at, finished = (lax.all_gather(both, axis, axis=dim, tiled=True), 0, [])
    for a in arrays:
        finished.append(lax.slice_in_dim(filled, at, at + a.shape[along], axis=along))
        at += a.shape[along]
    return tuple(finished)


def side_by_side_2(arrays, axis, split_dim, concat_dim, along):
    widths = [a.shape[along] for a in arrays]
    both = jnp.concatenate(arrays, axis=along)
    filled = lax.all_to_all(both, axis, split_axis=split_dim, concat_axis=concat_dim, tiled=True)
    return tuple(jnp.split(filled, [sum(widths[:k]) for k in range(1, len(widths))], axis=along))


def sent_to_all(x, axis):
    copies = jnp.broadcast_to(x, (lax.axis_size(axis), *x.shape))
    return lax.all_to_all(copies, axis, split_axis=0, concat_axis=0, tiled=True)


def all_in_one(x, axis):
    leaves = jax.tree.leaves(x)
    turns = sorted(range(len(leaves)), key=lambda k: -leaves[k].size)
    width = (1, *leaves[turns[0]].shape)[-1]
    lines = [
        jnp.pad(leaves[k].reshape(-1), (0, -leaves[k].size % width)).reshape(-1, width)
        for k in turns
    ]
    both, at, found = (sent_to_all(jnp.concatenate(lines), axis), 0, {})
    for k, line in zip(turns, lines):
        section = both[:, at : at + len(line)].reshape(len(both), -1)
        found[k] = section[:, : leaves[k].size].reshape(-1, *leaves[k].shape)
        at += len(line)
    numbers = iter(range(len(leaves)))
    return jax.tree.map(lambda _: found[next(numbers)], x)


def folded_in_pairs(pieces, combine):
    while len(jax.tree.leaves(pieces)[0]) > 1:
        pieces = jax.vmap(combine)(
            *(jax.tree.map(lambda part: part[side::2], pieces) for side in (0, 1))
        )
    return jax.tree.map(lambda part: part[0], pieces)


def entering(x, axis, combine, identity, reverse):
    length, index = (lax.axis_size(axis), lax.axis_index(axis))
    passed = jnp.arange(length) > index if reverse else jnp.arange(length) < index

    def kept(part, zero, own):
        part = jnp.where(
            passed.reshape(-1, *(1 for _ in own.shape)),
            part.astype(own.dtype),
            jnp.asarray(zero, own.dtype),
        )
        return part[::-1] if reverse else part

    pieces = all_in_one(
        jax.tree.map(
            lambda part, kind: part.astype(kind),
            x,
            jax.tree.map(lambda a: jnp.bfloat16 if a.dtype == jnp.float32 else a.dtype, x),
        ),
        axis,
    )
    return folded_in_pairs(jax.tree.map(kept, pieces, identity, x), combine)


def in_blocks(x, dim, length):
    lengths = x.shape
    blocks = x.reshape(*lengths[:dim], length, lengths[dim] // length, *lengths[dim + 1 :])
    return jnp.moveaxis(blocks, dim, 0)


def summed_on_arrival(x, axis, dim):
    length = lax.axis_size(axis)
    blocks = lax.all_to_all(in_blocks(x, dim, length), axis, 0, 0, tiled=True)
    return jnp.sum(blocks.astype(jnp.float32), axis=0)


def combine_spans(earlier, later):
    return (earlier[0] * later[0], later[1] + later[0][..., None] * earlier[1])


def contract_rows(left_mat, right_mat):
    return lax.dot_general(
        left_mat, right_mat, (((0,), (0,)), ((), ())), preferred_element_type=jnp.float32
    )


def contract_cols(left_mat, right_mat):
    return lax.dot_general(
        left_mat, right_mat, (((1,), (1,)), ((), ())), preferred_element_type=jnp.float32
    )


def to_blocks(tensor, head_count):
    rows_here = tensor.shape[0]
    return (
        tensor.astype(jnp.float32)
        .reshape(rows_here // BLOCK, BLOCK, head_count, -1)
        .transpose(2, 0, 1, 3)
    )


def from_blocks(tensor):
    head_count, blocks, _, channels = tensor.shape
    return tensor.transpose(1, 2, 0, 3).reshape(blocks * BLOCK, head_count * channels)


def expert_pass(rows_x, rows_cot, gate_mat, up_mat, down_mat):
    full_x, full_cot = side_by_side((rows_x, rows_cot), "tp", 1, 0)
    gate_pre = contract_cols(full_x, gate_mat)
    up_pre = contract_cols(full_x, up_mat)
    sigmoid_gate = jax.nn.sigmoid(gate_pre)
    active = gate_pre * sigmoid_gate
    hidden = (active * up_pre).astype(jnp.bfloat16)
    hidden_cot = contract_cols(full_cot, down_mat)
    up_cot = (hidden_cot * active).astype(jnp.bfloat16)
    gate_cot = (
        hidden_cot * up_pre * sigmoid_gate * (1.0 + gate_pre * (1.0 - sigmoid_gate))
    ).astype(jnp.bfloat16)
    down_g = contract_rows(hidden, full_cot)
    gate_g = contract_rows(gate_cot, full_x)
    up_g = contract_rows(up_cot, full_x)
    dims = (((0,), (1,)), ((), ()))
    first_part = lax.dot_general(gate_mat, gate_cot, dims, preferred_element_type=jnp.float32)
    back_terms = lax.psum_scatter(
        (
            first_part + lax.dot_general(up_mat, up_cot, dims, preferred_element_type=jnp.float32)
        ).astype(jnp.bfloat16),
        "tp",
        scatter_dimension=0,
        tiled=True,
    ).astype(jnp.float32)
    return (gate_g, up_g, down_g, back_terms)


def local(
    layer_in,
    out_cot,
    route_ids,
    route_probs,
    group_prob,
    gate_weight,
    up_weight,
    down_weight,
    out_weight,
    query,
    key_in,
    value,
    decay_logit,
):
    tok_rows = layer_in.shape[0]
    local_cols = layer_in.shape[1]
    experts_all = lax.axis_size("sp")
    capacity = 4 * tok_rows // experts_all
    route_weight = group_prob[:, None] * route_probs / jnp.sum(route_probs, axis=1, keepdims=True)
    chosen = (route_ids[:, :, None] == jnp.arange(experts_all, dtype=jnp.int32)).astype(jnp.int32)
    running = jnp.cumsum(chosen.reshape(2 * tok_rows, experts_all), axis=0).reshape(
        tok_rows, 2, experts_all
    )
    position = jnp.sum((running - 1) * chosen, axis=2)
    slot_ids = route_ids * capacity + position
    matches = (
        slot_ids[None, :, :] == jnp.arange(experts_all * capacity, dtype=jnp.int32)[:, None, None]
    )
    select_x = jnp.any(matches, axis=2).astype(jnp.float32)
    select_cot = jnp.sum(jnp.where(matches, route_weight[None], 0.0), axis=2)
    send_x = jnp.dot(
        select_x.astype(jnp.bfloat16), layer_in, preferred_element_type=jnp.float32
    ).astype(jnp.bfloat16)
    send_cot = jnp.dot(select_cot, out_cot.astype(jnp.float32), precision=highest).astype(
        jnp.bfloat16
    )
    send_x = send_x.reshape(experts_all, capacity, local_cols)
    send_cot = send_cot.reshape(experts_all, capacity, local_cols)
    recv_x, recv_cot = side_by_side_2((send_x, send_cot), "sp", 0, 0, 1)
    head_dev = query.shape[1] // DK
    scaled_query = to_blocks(query, head_dev) * DK ** (-0.5)
    key_blk = to_blocks(key_in, head_dev)
    value_blk = to_blocks(value, head_dev)
    logit_blk = to_blocks(decay_logit, head_dev)
    cumulative = jnp.cumsum(jax.nn.log_sigmoid(logit_blk) / decay_temp, axis=2)
    span_log = cumulative[:, :, -1:, :]
    growth = jnp.exp(cumulative)
    shrink = jnp.exp(-cumulative)
    to_end = jnp.exp(span_log - cumulative)
    query_decayed = scaled_query * growth
    key_back = key_blk * shrink
    key_to_end = key_blk * to_end
    causal = jnp.tril(jnp.ones((BLOCK, BLOCK), dtype=bool))
    scores = jnp.where(
        causal, jnp.einsum("hncd,hnsd->hncs", query_decayed, key_back, precision=highest), 0.0
    )
    within = jnp.einsum("hncs,hnsv->hncv", scores, value_blk, precision=highest)
    block_decay = jnp.moveaxis(jnp.exp(span_log[:, :, 0, :]), 1, 0)
    block_update = jnp.moveaxis(
        jnp.einsum("hncd,hncv->hndv", key_to_end, value_blk, precision=highest), 1, 0
    )
    identity_pair = (
        jnp.ones((head_dev, DK), jnp.float32),
        jnp.zeros((head_dev, DK, DV), jnp.float32),
    )

    def advance(carry_pair, inputs):
        return (combine_spans(carry_pair, inputs), carry_pair)

    span_total, before_pairs = lax.scan(advance, identity_pair, (block_decay, block_update))
    entry_pair = entering(span_total, "sp", combine_spans, identity_pair, False)
    entry_state = entry_pair[1]
    decay_before = jnp.moveaxis(before_pairs[0], 0, 1)
    block_state = decay_before[..., None] * entry_state[:, None] + jnp.moveaxis(
        before_pairs[1], 0, 1
    )
    span_end = span_total[0][..., None] * entry_state + span_total[1]
    outputs = within + jnp.einsum("hncd,hndv->hncv", query_decayed, block_state, precision=highest)
    mixer_out = from_blocks(outputs).astype(jnp.bfloat16)
    gate_mat, up_mat, down_mat = (gate_weight[0], up_weight[0], down_weight[0])
    gate_g, up_g, down_g, back_flat = expert_pass(
        recv_x.reshape(-1, local_cols), recv_cot.reshape(-1, local_cols), gate_mat, up_mat, down_mat
    )
    back_terms = back_flat.reshape(local_cols, experts_all, capacity)
    returned = lax.all_to_all(
        back_terms.astype(jnp.bfloat16), "sp", split_axis=1, concat_axis=1, tiled=True
    ).astype(back_terms.dtype)
    returned = returned.reshape(local_cols, experts_all * capacity)
    routed_sum = lax.dot_general(
        select_x,
        returned,
        (((0,), (1,)), ((), ())),
        precision=highest,
        preferred_element_type=jnp.float32,
    )
    mixed_cot = (out_cot.astype(jnp.float32) + routed_sum).astype(jnp.bfloat16)
    full_cot = lax.all_gather(mixed_cot, "tp", axis=1, tiled=True)
    mixer_cot = jnp.dot(full_cot, out_weight, preferred_element_type=jnp.float32)
    proj_grad = summed_on_arrival(contract_rows(full_cot, mixer_out).astype(jnp.bfloat16), "sp", 0)
    cot_blk = to_blocks(mixer_cot, head_dev)
    block_future = jnp.moveaxis(
        jnp.einsum("hncd,hncv->hndv", query_decayed, cot_blk, precision=highest), 1, 0
    )

    def retreat(carry_pair, inputs):
        return (combine_spans(carry_pair, inputs), carry_pair)

    span_back, after_pairs = lax.scan(
        retreat, identity_pair, (block_decay, block_future), reverse=True
    )
    beyond_pair = entering(span_back, "sp", combine_spans, identity_pair, True)
    future_state = beyond_pair[1]
    decay_after = jnp.moveaxis(after_pairs[0], 0, 1)
    block_future_state = decay_after[..., None] * future_state[:, None] + jnp.moveaxis(
        after_pairs[1], 0, 1
    )
    cot_values = jnp.where(
        causal, jnp.einsum("hncv,hnsv->hncs", cot_blk, value_blk, precision=highest), 0.0
    )
    query_scaled_grad = growth * (
        jnp.einsum("hncv,hndv->hncd", cot_blk, block_state, precision=highest)
        + jnp.einsum("hncs,hnsd->hncd", cot_values, key_back, precision=highest)
    )
    key_part = shrink * jnp.einsum("hncs,hncd->hnsd", cot_values, query_decayed, precision=highest)
    key_grad = key_part + to_end * jnp.einsum(
        "hnsv,hndv->hnsd", value_blk, block_future_state, precision=highest
    )
    value_grad = jnp.einsum("hncs,hncv->hnsv", scores, cot_blk, precision=highest) + jnp.einsum(
        "hnsd,hndv->hnsv", key_to_end, block_future_state, precision=highest
    )
    decay_terms = (scaled_query * query_scaled_grad - key_blk * key_grad).reshape(
        head_dev, tok_rows, DK
    )
    tail_sum = jnp.flip(jnp.cumsum(jnp.flip(decay_terms, 1), axis=1), 1)
    beyond_term = jnp.sum(future_state * span_end, axis=2)
    log_grad = tail_sum + beyond_term[:, None, :]
    logit_flat = logit_blk.reshape(head_dev, tok_rows, DK)
    logit_grad = (
        (log_grad * jax.nn.sigmoid(-logit_flat) / decay_temp)
        .transpose(1, 0, 2)
        .reshape(tok_rows, head_dev * DK)
    )
    query_grad = from_blocks(query_scaled_grad * DK ** (-0.5))
    return (
        gate_g[None],
        up_g[None],
        down_g[None],
        proj_grad,
        query_grad,
        from_blocks(key_grad),
        from_blocks(value_grad),
        logit_grad,
    )


def solution(mesh):
    in_specs = (
        P("sp", "tp"),
        P("sp", "tp"),
        P("sp", None),
        P("sp", None),
        P("sp"),
        P("sp", "tp", None),
        P("sp", "tp", None),
        P("sp", "tp", None),
        P(None, "tp"),
        P("sp", "tp"),
        P("sp", "tp"),
        P("sp", "tp"),
        P("sp", "tp"),
    )
    out_specs = (
        P("sp", "tp", None),
        P("sp", "tp", None),
        P("sp", "tp", None),
        P("sp", "tp"),
        P("sp", "tp"),
        P("sp", "tp"),
        P("sp", "tp"),
        P("sp", "tp"),
    )
    return jax.shard_map(local, mesh=mesh, in_specs=in_specs, out_specs=out_specs, check_vma=False)
```

profile of v0, /device:TPU:96, one launch (start us, length us, event | category | flops | bytes accessed | tf_op | source)
XLA Modules:
  0.0 298.2 jit_solution(3981683871783346753)
XLA Ops:
  7.2 0.9 copy.154
  8.4 1.4 reduce-window.14
  10.5 0.7 multiply_add_fusion.6
  11.6 0.7 reduce_sum.49
  12.3 0.7 multiply_divide_fusion
  13.5 2.7 convolution_convert_fusion.1
  16.1 1.4 convolution_convert_fusion.2
  17.5 19.8 %all_to_all.25 = bf16[16,160,128]{2,1,0:T(8,128)(2,1)S(1)} all-to-all(bf16[16,160,128]{2,1,0:T(8,128)(2,1)S(1)} %pad_maximum_fusion), channel_id=1, replica_groups=mesh['sp'=16,'tp'=16] {'sp'}, dimensions={0} | all-to-all | bytes 1310720 | tf_op jit(solution)/shard_map/all_to_all | solution.py:27
  37.4 0.9 pad_maximum_fusion.1
  38.5 68.6 %all-gather.3.cloned.1.call-done = bf16[2560,2048]{1,0:T(8,128)(2,1)} async-done(((bf16[2560,128]{1,0:T(8,128)(2,1)}), bf16[2560,2048]{1,0:T(8,128)(2,1)}) %all-gather.3.cloned.1.call-update) | async-done | bytes 10485776 | tf_op jit(solution)/shard_map/all_gather | solution.py:17
  107.2 4.2 %fusion.13 = f32[1280,128]{1,0:T(8,128)S(1)} fusion(bf16[2560,2048]{1,0:T(8,128)(2,1)} %all-gather.3.cloned.1.call-done, bf16[1,128,2048]{2,1,0:T(8,128)(2,1)S(1)} %copy-done), kind=kOutput, calls=%fused_computation.24 | convolution fusion | flops 671088640 | bytes 6422528 | tf_op jit(solution)/shard_map/dot_general | solution.py:107
  111.3 1.3 copy-done.1
  112.7 1.6 fusion.15
  114.3 1.7 multiply_convert_fusion.1
  116.0 1.5 fusion.33
  117.5 3.8 %fusion.4 = bf16[2048,1280]{0,1:T(8,128)(2,1)} fusion(f32[1280,2048]{1,0:T(8,128)S(1)} %fusion.33, bf16[1280,128]{1,0:T(8,128)(2,1)S(1)} %get-tuple-element.412, bf16[1,128,2048]{2,1,0:T(8,128)(2,1)S(1)} %copy-done.6), kind=kOutput, calls=%fused_computation.15 | convolution fusion | flops 676331520 | bytes 16580608 | tf_op jit(solution)/shard_map/dot_general | solution.py:145
  121.3 7.9 %copy.182 = bf16[2048,1280]{1,0:T(8,128)(2,1)} copy(bf16[2048,1280]{0,1:T(8,128)(2,1)} %fusion.4) | data formatting | bytes 10485760
  129.3 0.7 copy-done.8
  130.9 0.8 while.41
  131.9 0.8 broadcast_in_dim.136
  132.6 6.4 %all-to-all-start.2 = ((bf16[16,65,128]{2,1,0:T(8,128)(2,1)}), bf16[16,65,128]{2,1,0:T(8,128)(2,1)S(1)}, u32[]{:S(2)}, u32[]{:S(2)}) async-start(bf16[16,65,128]{2,1,0:T(8,128)(2,1)} %broadcast_in_dim.136), calls=%async_computation.2 | async-start | bytes 589824 | tf_op jit(solution)/shard_map/all_to_all | solution.py:33
  140.4 8.1 %all-to-all-done.2 = bf16[16,65,128]{2,1,0:T(8,128)(2,1)S(1)} async-done(((bf16[16,65,128]{2,1,0:T(8,128)(2,1)}), bf16[16,65,128]{2,1,0:T(8,128)(2,1)S(1)}, u32[]{:S(2)}, u32[]{:S(2)}) %all-to-all-start.2) | async-done | bytes 266272 | tf_op jit(solution)/shard_map/all_to_all | solution.py:33
  148.6 42.6 %reduce-scatter.4.cloned.1.call-done = bf16[128,1280]{1,0:T(8,128)(2,1)} async-done(((bf16[2048,1280]{1,0:T(8,128)(2,1)}), bf16[128,1280]{1,0:T(8,128)(2,1)}) %reduce-scatter.4.cloned.1.call-update) | async-done | bytes 327696
  191.3 1.9 copy.183
  193.1 6.5 %all-to-all-start.1 = ((bf16[128,16,80]{0,2,1:T(8,128)(2,1)}), bf16[128,16,80]{0,2,1:T(8,128)(2,1)}, u32[]{:S(2)}, u32[]{:S(2)}) async-start(bf16[128,16,80]{0,2,1:T(8,128)(2,1)} %bitcast.12), calls=%async_computation.1 | async-start | bytes 655360 | tf_op jit(solution)/shard_map/all_to_all | solution.py:239
  200.3 8.6 %all-to-all-done.1 = bf16[128,16,80]{0,2,1:T(8,128)(2,1)} async-done(((bf16[128,16,80]{0,2,1:T(8,128)(2,1)}), bf16[128,16,80]{0,2,1:T(8,128)(2,1)}, u32[]{:S(2)}, u32[]{:S(2)}) %all-to-all-start.1) | async-done | bytes 327712 | tf_op jit(solution)/shard_map/all_to_all | solution.py:239
  208.9 2.1 fusion.31
  211.4 1.0 fusion.30
  212.4 4.4 %fusion.18 = f32[1,128,2048]{2,1,0:T(8,128)} fusion(bf16[1280,128]{1,0:T(8,128)(2,1)S(1)} %get-tuple-element.413, bf16[2560,2048]{1,0:T(8,128)(2,1)} %all-gather.3.cloned.1.call-done), kind=kOutput, calls=%fused_computation.31 | convolution fusion | flops 671088640 | bytes 6619136 | tf_op jit(solution)/shard_map/dot_general | solution.py:101
  216.8 4.3 %fusion.21 = f32[1,128,2048]{2,1,0:T(8,128)} fusion(bf16[1280,128]{1,0:T(8,128)(2,1)S(1)} %get-tuple-element.412, bf16[2560,2048]{1,0:T(8,128)(2,1)} %all-gather.3.cloned.1.call-done), kind=kOutput, calls=%fused_computation.32 | convolution fusion | flops 671088640 | bytes 6619136 | tf_op jit(solution)/shard_map/dot_general | solution.py:101
  221.2 4.4 %fusion.24 = f32[1,128,2048]{2,1,0:T(8,128)} fusion(bf16[2560,2048]{1,0:T(8,128)(2,1)} %all-gather.3.cloned.1.call-done, f32[1280,128]{1,0:T(8,128)S(1)} %copy-done.20, f32[1280,128]{1,0:T(8,128)S(1)} %copy-done.18), kind=kOutput, calls=%fused_computation.33 | convolution fusion | flops 672071680 | bytes 7602176 | tf_op jit(solution)/shard_map/dot_general | solution.py:101
  225.6 21.5 %all-gather.5.cloned.1.call-done = bf16[320,2048]{1,0:T(8,128)(2,1)} async-done(((bf16[320,128]{1,0:T(8,128)(2,1)}), bf16[320,2048]{1,0:T(8,128)(2,1)}) %all-gather.5.cloned.1.call-update) | async-done | bytes 1310736 | tf_op jit(solution)/shard_map/all_gather | solution.py:251
  247.1 2.0 fusion.83
  249.1 1.1 fusion.46
  250.9 1.1 convolution_multiply_fusion
  252.1 7.3 %while.42 = (s32[]{:T(128)}, f32[1,64]{1,0:T(1,128)S(1)}, f32[1,64,128]{2,1,0:T(8,128)S(1)}, f32[5,1,64]{2,0,1:T(8,128)S(1)}, f32[5,1,64,128]{3,2,1,0:T(8,128)S(...) while((s32[]{:T(128)}, f32[1,64]{1,0:T(1,128)S(1)}, ...), condition=%wide.region_12.13_spmd.clone, body=%wide.region_11.12_spmd.clone.sunk | while | flops 32900 | bytes 166297 | solution.py:262
  252.1 0.7 fusion.122
  252.8 0.7 fusion.123
  253.5 0.7 fusion.122
  254.2 0.7 fusion.123
  255.0 0.7 fusion.122
  255.7 0.7 fusion.123
  256.4 0.7 fusion.122
  257.1 0.7 fusion.123
  257.9 0.7 fusion.122
  258.6 0.7 fusion.123
  259.4 0.7 broadcast_in_dim.141
  260.1 6.8 %all-to-all-start.4 = ((bf16[16,65,128]{2,1,0:T(8,128)(2,1)}), bf16[16,65,128]{2,1,0:T(8,128)(2,1)S(1)}, u32[]{:S(2)}, u32[]{:S(2)}) async-start(bf16[16,65,128]{2,1,0:T(8,128)(2,1)} %broadcast_in_dim.141), calls=%async_computation.4 | async-start | bytes 589824 | tf_op jit(solution)/shard_map/all_to_all | solution.py:33
  267.0 2.3 convolution_convert_fusion
  269.3 1.1 fusion.84
  270.4 1.9 fusion.29
  272.3 4.1 %all-to-all-done.4 = bf16[16,65,128]{2,1,0:T(8,128)(2,1)S(1)} async-done(((bf16[16,65,128]{2,1,0:T(8,128)(2,1)}), bf16[16,65,128]{2,1,0:T(8,128)(2,1)S(1)}, u32[]{:S(2)}, u32[]{:S(2)}) %all-to-all-start.4) | async-done | bytes 266272 | tf_op jit(solution)/shard_map/all_to_all | solution.py:33
  276.4 3.6 %all-to-all-start.3 = ((bf16[16,128,128]{2,1,0:T(8,128)(2,1)}), bf16[16,128,128]{2,1,0:T(8,128)(2,1)S(1)}, u32[]{:S(2)}, u32[]{:S(2)}) async-start(bf16[16,128,128]{2,1,0:T(8,128)(2,1)} %bitcast.35), calls=%async_computation.3 | async-start | bytes 1048576 | tf_op jit(solution)/shard_map/all_to_all | solution.py:92
  280.0 0.7 select_bitcast_fusion.2
  280.8 0.7 select_bitcast_fusion
  282.0 1.3 multiply_subtract_fusion
  283.8 0.9 reduce-window.16
  285.2 0.8 fusion.74
  286.0 0.8 copy.174
  286.8 0.8 copy.175
  287.8 0.8 fusion.55
  288.6 1.0 convolution_add_fusion.1
  289.6 1.4 all-to-all-done.3
  291.0 0.7 convert_reduce_fusion
  (182 shorter events, 9.1 us)
Async XLA Ops:
  7.2 100.0 %copy-start = (bf16[1,128,2048]{2,1,0:T(8,128)(2,1)S(1)}, bf16[1,128,2048]{2,1,0:T(8,128)(2,1)}, u32[]{:S(2)}) copy-start(bf16[1,128,2048]{2,1,0:T(8,128)(2,1)} %param.22) | copy-start | bytes 1572868
  7.2 100.0 %all-gather.3.cloned.1.call-start = ((), (), s32[]{:S(2)}) async-start(), calls=%async_computation.6 | async-start | bytes 11141120 | tf_op jit(solution)/shard_map/all_gather | solution.py:17
  11.6 26.6 %copy-start.7 = (pred[1280,320]{0,1:T(8,128)(4,1)}, pred[1280,320]{0,1:T(8,128)(4,1)S(1)}, u32[]{:S(2)}) copy-start(pred[1280,320]{0,1:T(8,128)(4,1)S(1)} %fusion.17) | copy-start | bytes 1228804
  38.3 73.1 %copy-start.6 = (bf16[1,128,2048]{2,1,0:T(8,128)(2,1)S(1)}, bf16[1,128,2048]{2,1,0:T(8,128)(2,1)}, u32[]{:S(2)}) copy-start(bf16[1,128,2048]{2,1,0:T(8,128)(2,1)} %param.23) | copy-start | bytes 1572868
  38.3 153.0 %reduce-scatter.4.cloned.1.call-start = ((), (), s32[]{:S(2)}) async-start(), calls=%async_computation.8 | async-start | bytes 5570560
  107.1 5.5 %copy-start.1 = (bf16[2560,2048]{1,0:T(8,128)(2,1)S(1)}, bf16[2560,2048]{1,0:T(8,128)(2,1)}, u32[]{:S(2)}) copy-start(bf16[2560,2048]{1,0:T(8,128)(2,1)} %all-gather.3.cloned.1.call-done) | copy-start | bytes 31457284
  112.7 1.6 copy-start.17
  112.7 1.6 copy-start.16
  114.3 1.7 copy-start.19
  129.2 0.8 copy-start.8
  129.2 0.9 copy-start.10
  129.2 1.3 copy-start.3
  129.2 9.8 %copy-start.9 = (bf16[320,64]{0,1:T(8,128)(2,1)S(1)}, bf16[320,64]{0,1:T(8,128)(2,1)}, u32[]{:S(2)}) copy-start(bf16[320,64]{0,1:T(8,128)(2,1)} %param.26) | copy-start | bytes 122884
  131.8 7.4 %copy-start.11 = (f32[5,1,64]{2,1,0:T(1,128)}, f32[5,1,64]{2,1,0:T(1,128)S(1)}, u32[]{:S(2)}) copy-start(f32[5,1,64]{2,1,0:T(1,128)S(1)} %get-tuple-element.589) | copy-start | bytes 3844
  131.8 79.4 %copy-start.12 = (f32[1,64]{1,0:T(1,128)}, f32[1,64]{1,0:T(1,128)S(1)}, u32[]{:S(2)}) copy-start(f32[1,64]{1,0:T(1,128)S(1)} %get-tuple-element.194) | copy-start | bytes 772
  132.6 15.9 %all-to-all-start.2 = ((bf16[16,65,128]{2,1,0:T(8,128)(2,1)}), bf16[16,65,128]{2,1,0:T(8,128)(2,1)S(1)}, u32[]{:S(2)}, u32[]{:S(2)}) async-start(bf16[16,65,128]{2,1,0:T(8,128)(2,1)} %broadcast_in_dim.136), calls=%async_computation.2 | async-start | bytes 589824 | tf_op jit(solution)/shard_map/all_to_all | solution.py:33
  193.1 15.8 %all-to-all-start.1 = ((bf16[128,16,80]{0,2,1:T(8,128)(2,1)}), bf16[128,16,80]{0,2,1:T(8,128)(2,1)}, u32[]{:S(2)}, u32[]{:S(2)}) async-start(bf16[128,16,80]{0,2,1:T(8,128)(2,1)} %bitcast.12), calls=%async_computation.1 | async-start | bytes 655360 | tf_op jit(solution)/shard_map/all_to_all | solution.py:239
  199.7 47.4 %all-gather.5.cloned.1.call-start = ((), (), s32[]{:S(2)}) async-start(), calls=%async_computation.7 | async-start | bytes 1392640 | tf_op jit(solution)/shard_map/all_gather | solution.py:251
  211.1 10.1 %copy-start.15 = (f32[64]{0:T(128)}, f32[64]{0:T(128)S(1)}, u32[]{:S(2)}) copy-start(f32[64]{0:T(128)S(1)} %slice_bitcast_fusion.1) | copy-start | bytes 772
  212.4 8.8 %copy-start.18 = (f32[1280,128]{1,0:T(8,128)S(1)}, f32[1280,128]{1,0:T(8,128)}, u32[]{:S(2)}) copy-start(f32[1280,128]{1,0:T(8,128)} %copy-done.17) | copy-start | bytes 1966084
  212.4 8.8 %copy-start.20 = (f32[1280,128]{1,0:T(8,128)S(1)}, f32[1280,128]{1,0:T(8,128)}, u32[]{:S(2)}) copy-start(f32[1280,128]{1,0:T(8,128)} %copy-done.19) | copy-start | bytes 1966084
  221.2 30.9 %copy-start.14 = (f32[1,64]{1,0:T(1,128)S(1)}, f32[1,64]{1,0:T(1,128)}, u32[]{:S(2)}) copy-start(f32[1,64]{1,0:T(1,128)} %custom-call.2) | copy-start | bytes 772
  247.1 19.9 %copy-start.2 = (bf16[320,2048]{1,0:T(8,128)(2,1)S(1)}, bf16[320,2048]{1,0:T(8,128)(2,1)}, u32[]{:S(2)}) copy-start(bf16[320,2048]{1,0:T(8,128)(2,1)} %all-gather.5.cloned.1.call-done) | copy-start | bytes 3932164
  260.1 16.2 %all-to-all-start.4 = ((bf16[16,65,128]{2,1,0:T(8,128)(2,1)}), bf16[16,65,128]{2,1,0:T(8,128)(2,1)S(1)}, u32[]{:S(2)}, u32[]{:S(2)}) async-start(bf16[16,65,128]{2,1,0:T(8,128)(2,1)} %broadcast_in_dim.141), calls=%async_computation.4 | async-start | bytes 589824 | tf_op jit(solution)/shard_map/all_to_all | solution.py:33
  267.0 18.3 %copy-start.13 = (f32[1,64]{1,0:T(1,128)S(1)}, f32[1,64]{1,0:T(1,128)}, u32[]{:S(2)}) copy-start(f32[1,64]{1,0:T(1,128)} %copy-done.12) | copy-start | bytes 772
  270.4 11.7 %copy-start.4 = (f32[5,64,64]{2,1,0:T(8,128)S(1)}, f32[5,64,64]{2,1,0:T(8,128)}, u32[]{:S(2)}) copy-start(f32[5,64,64]{2,1,0:T(8,128)} %convolution_multiply_fusion) | copy-start | bytes 245764
  276.4 14.6 %all-to-all-start.3 = ((bf16[16,128,128]{2,1,0:T(8,128)(2,1)}), bf16[16,128,128]{2,1,0:T(8,128)(2,1)S(1)}, u32[]{:S(2)}, u32[]{:S(2)}) async-start(bf16[16,128,128]{2,1,0:T(8,128)(2,1)} %bitcast.35), calls=%async_computation.3 | async-start | bytes 1048576 | tf_op jit(solution)/shard_map/all_to_all | solution.py:92
  281.5 7.0 %copy-start.5 = (f32[5,64,128]{2,1,0:T(8,128)S(1)}, f32[5,64,128]{2,1,0:T(8,128)}, u32[]{:S(2)}) copy-start(f32[5,64,128]{2,1,0:T(8,128)} %fusion.84) | copy-start | bytes 491524
Sparse Core Ops, SparseCore 0:
  38.4 68.7 all-gather.2
  129.4 61.8 reduce-scatter.3
  211.2 35.8 all-gather.4
where the time goes:
time: 301 us; the launch traced here: 298 us
  waiting for transfers between devices  155 us (51%)
  matrix products  46.6 us (15%)
  starting transfers between devices  23.8 us (8%)
  local copies, waits for them, and re-layouts  22.1 us (7%)
  blocking collectives  19.8 us (7%)
  other arithmetic  16.2 us (5%)
  between operations  14.5 us (5%)
    all_gather x1, waiting for transfers between devices, side_by_side(): lax.all_gather(both, axis, axis=dim, tiled=True)  68.6 us
    unnamed x4, waiting for transfers between devices  42.7 us
    all_gather x1, waiting for transfers between devices, local(): full_cot = lax.all_gather(mixed_cot, 'tp', axis=1, tiled=True)  21.5 us
    all_to_all x1, blocking collectives, side_by_side_2(): lax.all_to_all(both, axis, split_axis=split_dim, concat_axis=concat_dim,...  19.8 us
    dot_general x4, matrix products, contract_rows(): lax.dot_general(left_mat, right_mat, (((0,), (0,)), ((), ())), preferred_...  15.5 us
    unnamed x52, local copies, waits for them, and re-layouts  14.8 us
    all_to_all x2, starting transfers between devices, sent_to_all(): return lax.all_to_all(copies, axis, split_axis=0, concat_axis=0, tiled=True)  13.2 us
    all_to_all x2, waiting for transfers between devices, sent_to_all(): return lax.all_to_all(copies, axis, split_axis=0, concat_axis=0, tiled=True)  12.1 us
  transfers between devices with their start and end apart: 7, of which 7 were waited for; matrix products, arithmetic and copies ran while one was open for 11% of the time, Pallas kernels for 0%

commit v1 on v0

--- a/solution.py
+++ b/solution.py
@@ -1,6 +1,10 @@
+import functools
+
 import jax
 import jax.numpy as jnp
 from jax import lax
+from jax.experimental import pallas as pl
+from jax.experimental.pallas import tpu as pltpu
 from jax.sharding import PartitionSpec as P
 
 DK = 64
@@ -10,22 +14,524 @@
 
 decay_temp = 16.0
 highest = lax.Precision.HIGHEST
-
-
-def side_by_side(arrays, axis, dim, along):
-    both = jnp.concatenate(arrays, axis=along)
-    filled, at, finished = (lax.all_gather(both, axis, axis=dim, tiled=True), 0, [])
-    for a in arrays:
-        finished.append(lax.slice_in_dim(filled, at, at + a.shape[along], axis=along))
-        at += a.shape[along]
-    return tuple(finished)
-
-
-def side_by_side_2(arrays, axis, split_dim, concat_dim, along):
-    widths = [a.shape[along] for a in arrays]
-    both = jnp.concatenate(arrays, axis=along)
-    filled = lax.all_to_all(both, axis, split_axis=split_dim, concat_axis=concat_dim, tiled=True)
-    return tuple(jnp.split(filled, [sum(widths[:k]) for k in range(1, len(widths))], axis=along))
+f32, bf16 = jnp.float32, jnp.bfloat16
+MESH = pl.DeviceIdType.MESH
+
+
+def dot_nt(a, b):
+    return lax.dot_general(a, b, (((1,), (1,)), ((), ())), preferred_element_type=f32)
+
+
+def dot_nn(a, b):
+    return lax.dot_general(a, b, (((1,), (0,)), ((), ())), preferred_element_type=f32)
+
+
+def moe_kernel(
+    sizes,
+    layer_in,
+    out_cot,
+    ids,
+    probs,
+    group,
+    gate,
+    up,
+    down,
+    out_w,
+    gate_g,
+    up_g,
+    down_g,
+    full_cot,
+    mixer_cot,
+    send,
+    sel_t,
+    rows,
+    pre,
+    part_w,
+    gu,
+    gu_part,
+    gu_t,
+    hid_t,
+    stage,
+    inbox,
+    ret_out,
+    ret,
+    a2a_s,
+    a2a_r,
+    back_s,
+    back_r,
+    ag_s,
+    ag_r,
+    agd_s,
+    agd_r,
+    rs_s,
+    rs_r,
+    tk_s,
+    tk_r,
+    tkd_s,
+    tkd_r,
+    misc_s,
+    misc_r,
+):
+    n_sp, n_x, n_z, pieces = sizes
+    n_y = n_sp // n_x
+    half = n_z // 2
+    toks, cols = layer_in.shape
+    cap = 4 * toks // n_sp
+    n_rows = n_sp * cap
+    per = n_sp // pieces
+    chunk = n_rows // pieces
+    sp = lax.axis_index("sp")
+    tp = lax.axis_index("tp")
+    core = lax.rem(tp, 2)
+    z = tp // 2
+    z_up = lax.rem(z + 1, n_z)
+    z_dn = lax.rem(z + n_z - 1, n_z)
+    partner = (sp, 2 * z + 1 - core)
+    above, below = (sp, 2 * z_up + core), (sp, 2 * z_dn + core)
+    my_y, my_x = sp // n_x, lax.rem(sp, n_x)
+
+    def there(r):
+        ry, rx = r // n_x, lax.rem(r, n_x)
+        return lax.rem(my_y + ry, n_y) * n_x + lax.rem(my_x + rx, n_x)
+
+    def back_to(r):
+        ry, rx = r // n_x, lax.rem(r, n_x)
+        return lax.rem(my_y + n_y - ry, n_y) * n_x + lax.rem(my_x + n_x - rx, n_x)
+
+    def zpos(d):
+        return lax.rem(z + d + n_z, n_z)
+
+    def remote(src, dst, s, r, dev):
+        return pltpu.make_async_remote_copy(
+            src_ref=src, dst_ref=dst, send_sem=s, recv_sem=r, device_id=dev, device_id_type=MESH
+        )
+
+    barrier = pltpu.get_barrier_semaphore()
+    for r in range(1, n_sp):
+        pl.semaphore_signal(barrier, inc=1, device_id=(there(r), tp), device_id_type=MESH)
+    for dev in (partner, above, below):
+        pl.semaphore_signal(barrier, inc=1, device_id=dev, device_id_type=MESH)
+
+    experts = lax.broadcasted_iota(jnp.int32, (toks, 128), 1)
+    id0, id1 = ids[:, 0:1], ids[:, 1:2]
+    hit0, hit1 = experts == id0, experts == id1
+    chosen = (jnp.where(hit0, 1.0, 0.0) + jnp.where(hit1, 1.0, 0.0)).astype(bf16)
+    t_row = lax.broadcasted_iota(jnp.int32, (toks, toks), 0)
+    t_col = lax.broadcasted_iota(jnp.int32, (toks, toks), 1)
+    earlier = jnp.where(t_col < t_row, 1.0, 0.0).astype(bf16)
+    count = dot_nn(earlier, chosen)
+    pos0 = jnp.sum(jnp.where(hit0, count, 0.0), axis=1, keepdims=True)
+    pos1 = jnp.sum(jnp.where(hit1, count, 0.0), axis=1, keepdims=True)
+
+    def offset_of(expert):
+        ey, ex = expert // n_x, lax.rem(expert, n_x)
+        return lax.rem(ey + n_y - my_y, n_y) * n_x + lax.rem(ex + n_x - my_x, n_x)
+
+    slot0 = offset_of(id0) * cap + pos0.astype(jnp.int32)
+    slot1 = offset_of(id1) * cap + pos1.astype(jnp.int32)
+    slots = lax.broadcasted_iota(jnp.int32, (toks, n_rows), 1)
+    sel_t[...] = (
+        jnp.where(slots == slot0, 1.0, 0.0) + jnp.where(slots == slot1, 1.0, 0.0)
+    ).astype(bf16)
+    diagonal = t_row == t_col
+
+    def as_row(column):
+        return jnp.sum(jnp.where(diagonal, column, 0.0), axis=0, keepdims=True)
+
+    p0, p1 = as_row(probs[:, 0:1]), as_row(probs[:, 1:2])
+    w0 = group[...] * p0 / (p0 + p1)
+    w1 = group[...] * p1 / (p0 + p1)
+    slot0_row, slot1_row = as_row(slot0.astype(f32)), as_row(slot1.astype(f32))
+    both = jnp.concatenate([layer_in[...], out_cot[...]], axis=1)
+
+    def select(p, carry):
+        base = pl.multiple_of(p * chunk, chunk)
+        here = (lax.broadcasted_iota(jnp.int32, (chunk, toks), 0) + p * chunk).astype(f32)
+        m0, m1 = here == slot0_row, here == slot1_row
+        pick = (jnp.where(m0, 1.0, 0.0) + jnp.where(m1, 1.0, 0.0)).astype(bf16)
+        weight = jnp.sum(jnp.where(m0, w0, 0.0) + jnp.where(m1, w1, 0.0), axis=1, keepdims=True)
+        picked = dot_nn(pick, both)
+        send[0, pl.ds(base, chunk), :] = picked[:, :cols].astype(bf16)
+        send[1, pl.ds(base, chunk), :] = (picked[:, cols:] * weight).astype(bf16)
+        return carry
+
+    lax.fori_loop(0, pieces, select, 0)
+    pl.semaphore_wait(barrier, n_sp + 2)
+
+    give_w = [
+        remote(w, part_w.at[k], misc_s.at[k], misc_r.at[k], partner)
+        for k, w in enumerate((gate, up))
+    ]
+    for copy in give_w:
+        copy.start()
+
+    def slot_rows(r):
+        return pl.ds(pl.multiple_of(r * cap, cap), cap)
+
+    def dispatch(r):
+        return remote(
+            send.at[:, slot_rows(r), :],
+            rows.at[tp, :, slot_rows(r), :],
+            a2a_s.at[r],
+            a2a_r.at[r],
+            (there(r), tp),
+        )
+
+    def start_dispatch(r, carry):
+        dispatch(r).start()
+        return carry
+
+    lax.fori_loop(1, n_sp, start_dispatch, 0)
+    rows[tp, :, slot_rows(0), :] = send[:, slot_rows(0), :]
+
+    last = (half - 1) * pieces
+
+    def ring(n_pieces, where, sems_s, sems_r, sems_ds, sems_dr, own_ready, compute):
+        h_p = n_pieces // 2
+        total = (half - 1) * n_pieces + h_p
+
+        def along(block, p, d, k):
+            ref = where(block, p)
+            return remote(ref, ref, sems_s.at[d, k], sems_r.at[d, k], above if d == 0 else below)
+
+        def across(block, p, k):
+            ref = where(block, p)
+            return remote(ref, ref, sems_ds.at[k], sems_dr.at[k], partner)
+
+        def own(p, carry):
+            own_ready(p)
+            along(tp, p, 0, p).start()
+            along(tp, p, 1, p).start()
+            across(tp, p, p).start()
+            return carry
+
+        lax.fori_loop(0, n_pieces, own, 0)
+
+        def own_compute(p, carry):
+            across(tp, p, p).wait_recv()
+            compute(z, p)
+            return carry
+
+        lax.fori_loop(0, n_pieces, own_compute, 0)
+
+        def at(t):
+            in_half = t >= (half - 1) * n_pieces
+            p_up = lax.rem(t, n_pieces)
+            p_dn = jnp.where(in_half, p_up + h_p, p_up)
+            hop = t // n_pieces
+            return hop, p_up, p_dn
+
+        def step(t, carry):
+            hop, p_up, p_dn = at(t)
+            b_up, b_dn = zpos(-1 - hop), zpos(1 + hop)
+            along(2 * b_up + core, p_up, 0, t).wait_recv()
+
+            @pl.when((hop < half - 2) | ((hop == half - 2) & (p_up < h_p)))
+            def _():
+                along(2 * b_up + core, p_up, 0, t + n_pieces).start()
+
+            across(2 * b_up + core, p_up, n_pieces + 2 * t).start()
+            along(2 * b_dn + core, p_dn, 1, t).wait_recv()
+
+            @pl.when(hop < half - 2)
+            def _():
+                along(2 * b_dn + core, p_dn, 1, t + n_pieces).start()
+
+            @pl.when((hop == half - 2) & (p_dn >= h_p))
+            def _():
+                along(2 * b_dn + core, p_dn, 1, t + n_pieces - h_p).start()
+
+            across(2 * b_dn + core, p_dn, n_pieces + 2 * t + 1).start()
+
+            @pl.when(t > 0)
+            def _():
+                use(t - 1)
+
+            return carry
+
+        def use(t):
+            hop, p_up, p_dn = at(t)
+            b_up, b_dn = zpos(-1 - hop), zpos(1 + hop)
+            across(2 * b_up + 1 - core, p_up, n_pieces + 2 * t).wait_recv()
+            compute(b_up, p_up)
+            across(2 * b_dn + 1 - core, p_dn, n_pieces + 2 * t + 1).wait_recv()
+            compute(b_dn, p_dn)
+
+        lax.fori_loop(0, total, step, 0)
+        use(total - 1)
+
+        def drain():
+            def one(k, carry):
+                along(tp, 0, 0, k).wait_send()
+                along(tp, 0, 1, k).wait_send()
+                return carry
+
+            lax.fori_loop(0, total, one, 0)
+
+            def other(k, carry):
+                across(tp, 0, k).wait_send()
+                return carry
+
+            lax.fori_loop(0, n_pieces + 2 * total, other, 0)
+
+        return drain
+
+    def piece_rows(p):
+        return pl.ds(pl.multiple_of(p * chunk, chunk), chunk)
+
+    def rows_ready(p):
+        for i in range(per):
+            r = p * per + i
+
+            @pl.when(r > 0)
+            def _():
+                dispatch(r).wait_recv()
+
+    def feats(b):
+        return pl.ds(pl.multiple_of(b * 2 * cols, 2 * cols), 2 * cols)
+
+    pre[...] = jnp.zeros_like(pre)
+
+    def expert_in(b, p):
+        w_gu = jnp.concatenate([gate[:, feats(b)], up[:, feats(b)]], axis=0)
+        at = piece_rows(p)
+        x = jnp.concatenate([rows[2 * b, 0, at, :], rows[2 * b + 1, 0, at, :]], axis=1)
+        c = jnp.concatenate([rows[2 * b, 1, at, :], rows[2 * b + 1, 1, at, :]], axis=1)
+        pre[at, 0:256] += dot_nt(x, w_gu)
+        pre[at, 256:384] += dot_nt(c, down[:, feats(b)])
+
+    drain_rows = ring(
+        pieces,
+        lambda block, p: rows.at[block, :, piece_rows(p), :],
+        ag_s,
+        ag_r,
+        agd_s,
+        agd_r,
+        rows_ready,
+        expert_in,
+    )
+
+    def middle(p, carry):
+        at = piece_rows(p)
+        gate_pre, up_pre, hidden_cot = pre[at, 0:128], pre[at, 128:256], pre[at, 256:384]
+        sig = jax.nn.sigmoid(gate_pre)
+        active = gate_pre * sig
+        hidden = active * up_pre
+        up_cot = (hidden_cot * active).astype(bf16)
+        gate_cot = (hidden_cot * up_pre * sig * (1.0 + gate_pre * (1.0 - sig))).astype(bf16)
+        gu[at, 0:128] = gate_cot
+        gu[at, 128:256] = up_cot
+        pre[at, 0:128] = hidden
+        return carry
+
+    lax.fori_loop(0, pieces, middle, 0)
+    give_gu = remote(gu, gu_part, misc_s.at[2], misc_r.at[2], partner)
+    give_gu.start()
+    gu_t[...] = gu[...].T
+    hid_t[...] = pre[:, 0:128].astype(bf16).T
+    for copy in give_w:
+        copy.wait_recv()
+    give_gu.wait_recv()
+
+    h_p = pieces // 2
+    rs_total = h_p + (half - 1) * pieces
+
+    def partial(b, p):
+        cols_at = pl.ds(pl.multiple_of((2 * b + core) * cols, cols), cols)
+        mine = jnp.concatenate([gate[:, cols_at], up[:, cols_at]], axis=0)
+        theirs = jnp.concatenate([part_w[0, :, cols_at], part_w[1, :, cols_at]], axis=0)
+        at = piece_rows(p)
+        return dot_nn(gu[at, :], mine) + dot_nn(gu_part[at, :], theirs)
+
+    def hop_sum(d, k):
+        return remote(
+            stage.at[d, k],
+            inbox.at[d, k],
+            rs_s.at[d, k],
+            rs_r.at[d, k],
+            above if d == 0 else below,
+        )
+
+    def first(t, carry):
+        for d in range(2):
+            stage[d, t] = partial(zpos(half), t + d * h_p).astype(bf16)
+            hop_sum(d, t).start()
+        return carry
+
+    lax.fori_loop(0, h_p, first, 0)
+
+    def gradients(b):
+        x = jnp.concatenate([rows[2 * b, 0], rows[2 * b + 1, 0]], axis=1)
+        c = jnp.concatenate([rows[2 * b, 1], rows[2 * b + 1, 1]], axis=1)
+        both_g = dot_nn(gu_t[...], x)
+        gate_g[:, feats(b)] = both_g[0:128]
+        up_g[:, feats(b)] = both_g[128:256]
+        down_g[:, feats(b)] = dot_nn(hid_t[...], c)
+
+    def later(u, carry):
+        t = u + h_p
+        hop, p = 1 + u // pieces, lax.rem(u, pieces)
+        for d in range(2):
+            dest = zpos(half - hop) if d == 0 else zpos(hop - half)
+            value = partial(dest, p)
+            mine_first = (p >= h_p) if d == 0 else (p < h_p)
+            alone = (hop == 1) & mine_first
+            k_in = jnp.where(hop == 1, p - d * h_p, t - pieces)
+
+            @pl.when(alone)
+            def _():
+                stage[d, t] = value.astype(bf16)
+
+            @pl.when(jnp.logical_not(alone))
+            def _():
+                hop_sum(d, k_in).wait_recv()
+                stage[d, t] = (value + inbox[d, k_in].astype(f32)).astype(bf16)
+
+            hop_sum(d, t).start()
+
+        @pl.when(u < n_z)
+        def _():
+            gradients(u)
+
+        return carry
+
+    lax.fori_loop(0, rs_total - h_p, later, 0)
+
+    def give_back(r):
+        return remote(
+            ret_out.at[slot_rows(r), :],
+            ret.at[slot_rows(r), :],
+            back_s.at[r],
+            back_r.at[r],
+            (back_to(r), tp),
+        )
+
+    def finish(p, carry):
+        k_in = rs_total - pieces + p
+        value = partial(z, p)
+        for d in range(2):
+            hop_sum(d, k_in).wait_recv()
+            value = value + inbox[d, k_in].astype(f32)
+        ret_out[piece_rows(p), :] = value.astype(bf16)
+        for i in range(per):
+            r = p * per + i
+
+            @pl.when(r > 0)
+            def _():
+                give_back(r).start()
+
+        return carry
+
+    lax.fori_loop(0, pieces, finish, 0)
+    for g in range(rs_total - h_p, n_z):
+        gradients(g)
+    ret[slot_rows(0), :] = ret_out[slot_rows(0), :]
+
+    def take_back(r, carry):
+        give_back(r).wait_recv()
+        return carry
+
+    lax.fori_loop(1, n_sp, take_back, 0)
+    mixed = (out_cot[...].astype(f32) + dot_nn(sel_t[...], ret[...])).astype(bf16)
+    full_cot[tp] = mixed
+
+    tok_half = toks // 2
+    mixer_cot[...] = jnp.zeros_like(mixer_cot)
+
+    def project(b, p):
+        at = pl.ds(pl.multiple_of(p * tok_half, tok_half), tok_half)
+        c = jnp.concatenate([full_cot[2 * b, at, :], full_cot[2 * b + 1, at, :]], axis=1)
+        mixer_cot[at, :] += dot_nn(c, out_w[feats(b), :])
+
+    drain_toks = ring(
+        2,
+        lambda block, p: full_cot.at[block, pl.ds(pl.multiple_of(p * tok_half, tok_half), tok_half), :],
+        tk_s,
+        tk_r,
+        tkd_s,
+        tkd_r,
+        lambda p: None,
+        project,
+    )
+
+    def sent(r, carry):
+        dispatch(r).wait_send()
+        give_back(r).wait_send()
+        return carry
+
+    lax.fori_loop(1, n_sp, sent, 0)
+    for copy in (*give_w, give_gu):
+        copy.wait_send()
+
+    def sums_sent(k, carry):
+        for d in range(2):
+            hop_sum(d, k).wait_send()
+        return carry
+
+    lax.fori_loop(0, rs_total, sums_sent, 0)
+    drain_rows()
+    drain_toks()
+
+
+def moe(layer_in, out_cot, ids, probs, group, gate, up, down, out_w, n_sp, n_tp):
+    toks, cols = layer_in.shape
+    n_x = 4 if n_sp == 16 else n_sp
+    n_z = n_tp // 2
+    half = n_z // 2
+    pieces = 4 if n_sp % 4 == 0 else 2
+    width = gate.shape[1]
+    n_rows = 4 * toks
+    total = (half - 1) * pieces + pieces // 2
+    tk_total = (half - 1) * 2 + 1
+    chunk = n_rows // pieces
+    dma = pltpu.SemaphoreType.DMA
+    vmem = pl.BlockSpec(memory_space=pltpu.VMEM)
+    return pl.pallas_call(
+        functools.partial(moe_kernel, (n_sp, n_x, n_z, pieces)),
+        out_shape=(
+            jax.ShapeDtypeStruct((128, width), f32),
+            jax.ShapeDtypeStruct((128, width), f32),
+            jax.ShapeDtypeStruct((128, width), f32),
+            jax.ShapeDtypeStruct((n_tp, toks, cols), bf16),
+            jax.ShapeDtypeStruct((toks, 128), f32),
+        ),
+        in_specs=[vmem] * 9,
+        out_specs=[vmem] * 5,
+        scratch_shapes=[
+            pltpu.VMEM((2, n_rows, cols), bf16),
+            pltpu.VMEM((toks, n_rows), bf16),
+            pltpu.VMEM((n_tp, 2, n_rows, cols), bf16),
+            pltpu.VMEM((n_rows, 384), f32),
+            pltpu.VMEM((2, 128, width), bf16),
+            pltpu.VMEM((n_rows, 256), bf16),
+            pltpu.VMEM((n_rows, 256), bf16),
+            pltpu.VMEM((256, n_rows), bf16),
+            pltpu.VMEM((128, n_rows), bf16),
+            pltpu.VMEM((2, total, chunk, cols), bf16),
+            pltpu.VMEM((2, total, chunk, cols), bf16),
+            pltpu.VMEM((n_rows, cols), bf16),
+            pltpu.VMEM((n_rows, cols), bf16),
+            dma((n_sp,)),
+            dma((n_sp,)),
+            dma((n_sp,)),
+            dma((n_sp,)),
+            dma((2, total)),
+            dma((2, total)),
+            dma((pieces + 2 * total,)),
+            dma((pieces + 2 * total,)),
+            dma((2, total)),
+            dma((2, total)),
+            dma((2, tk_total)),
+            dma((2, tk_total)),
+            dma((2 + 2 * tk_total,)),
+            dma((2 + 2 * tk_total,)),
+            dma((3,)),
+            dma((3,)),
+        ],
+        compiler_params=pltpu.CompilerParams(
+            collective_id=0, has_side_effects=True, vmem_limit_bytes=60 * 1024 * 1024
+        ),
+    )(layer_in, out_cot, ids, probs, group, gate, up, down, out_w)
 
 
 def sent_to_all(x, axis):
@@ -121,34 +627,6 @@
 def from_blocks(tensor):
     head_count, blocks, _, channels = tensor.shape
     return tensor.transpose(1, 2, 0, 3).reshape(blocks * BLOCK, head_count * channels)
-
-
-def expert_pass(rows_x, rows_cot, gate_mat, up_mat, down_mat):
-    full_x, full_cot = side_by_side((rows_x, rows_cot), "tp", 1, 0)
-    gate_pre = contract_cols(full_x, gate_mat)
-    up_pre = contract_cols(full_x, up_mat)
-    sigmoid_gate = jax.nn.sigmoid(gate_pre)
-    active = gate_pre * sigmoid_gate
-    hidden = (active * up_pre).astype(jnp.bfloat16)
-    hidden_cot = contract_cols(full_cot, down_mat)
-    up_cot = (hidden_cot * active).astype(jnp.bfloat16)
-    gate_cot = (
-        hidden_cot * up_pre * sigmoid_gate * (1.0 + gate_pre * (1.0 - sigmoid_gate))
-    ).astype(jnp.bfloat16)
-    down_g = contract_rows(hidden, full_cot)
-    gate_g = contract_rows(gate_cot, full_x)
-    up_g = contract_rows(up_cot, full_x)
-    dims = (((0,), (1,)), ((), ()))
-    first_part = lax.dot_general(gate_mat, gate_cot, dims, preferred_element_type=jnp.float32)
-    back_terms = lax.psum_scatter(
-        (
-            first_part + lax.dot_general(up_mat, up_cot, dims, preferred_element_type=jnp.float32)
-        ).astype(jnp.bfloat16),
-        "tp",
-        scatter_dimension=0,
-        tiled=True,
-    ).astype(jnp.float32)
-    return (gate_g, up_g, down_g, back_terms)
 
 
 def local(
@@ -167,30 +645,6 @@
     decay_logit,
 ):
     tok_rows = layer_in.shape[0]
-    local_cols = layer_in.shape[1]
-    experts_all = lax.axis_size("sp")
-    capacity = 4 * tok_rows // experts_all
-    route_weight = group_prob[:, None] * route_probs / jnp.sum(route_probs, axis=1, keepdims=True)
-    chosen = (route_ids[:, :, None] == jnp.arange(experts_all, dtype=jnp.int32)).astype(jnp.int32)
-    running = jnp.cumsum(chosen.reshape(2 * tok_rows, experts_all), axis=0).reshape(
-        tok_rows, 2, experts_all
-    )
-    position = jnp.sum((running - 1) * chosen, axis=2)
-    slot_ids = route_ids * capacity + position
-    matches = (
-        slot_ids[None, :, :] == jnp.arange(experts_all * capacity, dtype=jnp.int32)[:, None, None]
-    )
-    select_x = jnp.any(matches, axis=2).astype(jnp.float32)
-    select_cot = jnp.sum(jnp.where(matches, route_weight[None], 0.0), axis=2)
-    send_x = jnp.dot(
-        select_x.astype(jnp.bfloat16), layer_in, preferred_element_type=jnp.float32
-    ).astype(jnp.bfloat16)
-    send_cot = jnp.dot(select_cot, out_cot.astype(jnp.float32), precision=highest).astype(
-        jnp.bfloat16
-    )
-    send_x = send_x.reshape(experts_all, capacity, local_cols)
-    send_cot = send_cot.reshape(experts_all, capacity, local_cols)
-    recv_x, recv_cot = side_by_side_2((send_x, send_cot), "sp", 0, 0, 1)
     head_dev = query.shape[1] // DK
     scaled_query = to_blocks(query, head_dev) * DK ** (-0.5)
     key_blk = to_blocks(key_in, head_dev)
@@ -231,26 +685,23 @@
     span_end = span_total[0][..., None] * entry_state + span_total[1]
     outputs = within + jnp.einsum("hncd,hndv->hncv", query_decayed, block_state, precision=highest)
     mixer_out = from_blocks(outputs).astype(jnp.bfloat16)
-    gate_mat, up_mat, down_mat = (gate_weight[0], up_weight[0], down_weight[0])
-    gate_g, up_g, down_g, back_flat = expert_pass(
-        recv_x.reshape(-1, local_cols), recv_cot.reshape(-1, local_cols), gate_mat, up_mat, down_mat
-    )
-    back_terms = back_flat.reshape(local_cols, experts_all, capacity)
-    returned = lax.all_to_all(
-        back_terms.astype(jnp.bfloat16), "sp", split_axis=1, concat_axis=1, tiled=True
-    ).astype(back_terms.dtype)
-    returned = returned.reshape(local_cols, experts_all * capacity)
-    routed_sum = lax.dot_general(
-        select_x,
-        returned,
-        (((0,), (1,)), ((), ())),
-        precision=highest,
-        preferred_element_type=jnp.float32,
-    )
-    mixed_cot = (out_cot.astype(jnp.float32) + routed_sum).astype(jnp.bfloat16)
-    full_cot = lax.all_gather(mixed_cot, "tp", axis=1, tiled=True)
-    mixer_cot = jnp.dot(full_cot, out_weight, preferred_element_type=jnp.float32)
-    proj_grad = summed_on_arrival(contract_rows(full_cot, mixer_out).astype(jnp.bfloat16), "sp", 0)
+    n_sp, n_tp = lax.axis_size("sp"), lax.axis_size("tp")
+    gate_g, up_g, down_g, full_cot, mixer_cot = moe(
+        layer_in,
+        out_cot,
+        route_ids,
+        route_probs,
+        group_prob.reshape(1, tok_rows),
+        gate_weight[0],
+        up_weight[0],
+        down_weight[0],
+        out_weight,
+        n_sp,
+        n_tp,
+    )
+    proj_part = jnp.einsum("btf,tv->bfv", full_cot, mixer_out, preferred_element_type=f32)
+    proj_all = lax.all_to_all(proj_part.astype(bf16), "sp", 0, 0, tiled=True)
+    proj_grad = jnp.sum(proj_all.astype(f32), axis=0)
     cot_blk = to_blocks(mixer_cot, head_dev)
     block_future = jnp.moveaxis(
         jnp.einsum("hncd,hncv->hndv", query_decayed, cot_blk, precision=highest), 1, 0

time: 301 us -> 185 us (0.61)
  waiting for transfers between devices: 155 us -> 20.9 us
  Pallas kernels: 0 us -> 122 us
  matrix products: 46.6 us -> 7.41 us
  blocking collectives: 19.8 us -> 0 us
  between operations: 14.5 us -> 1.4 us
  starting transfers between devices: 23.8 us -> 11.8 us
  local copies, waits for them, and re-layouts: 22.1 us -> 12.8 us
  other arithmetic: 16.2 us -> 7.39 us
    pallas_call x0 -> x1, Pallas kernels: none -> 122 us  [moe(): pl.pallas_call(functools.partial(moe_kernel, (n_sp, n_x, n_z, pieces)), o...]
    all_gather x2 -> x0, waiting for transfers between devices: 90.1 us -> none  [the longest x1 68.6 us: side_by_side(): lax.all_gather(both, axis, axis=dim, tiled=True)]
    unnamed x4 -> x0, waiting for transfers between devices: 42.7 us -> none
    dot_general x13 -> x1, matrix products: 36.4 us -> 1.43 us  [local(): jnp.einsum('btf,tv->bfv', full_cot, mixer_out, preferred_element_type=f32)]
    all_to_all x1 -> x0, blocking collectives: 19.8 us -> none  [side_by_side_2(): lax.all_to_all(both, axis, split_axis=split_dim, concat_axis=concat_dim,...]
    all_to_all x2 -> x1, starting transfers between devices: 10.1 us -> 3.72 us  [local(): proj_all = lax.all_to_all(proj_part.astype(bf16), 'sp', 0, 0, tiled=True)]
    unnamed x52 -> x68, local copies, waits for them, and re-layouts: 14.8 us -> 8.9 us
    all_to_all x2, starting transfers between devices: 13.2 us -> 8.07 us  [sent_to_all(): return lax.all_to_all(copies, axis, split_axis=0, concat_axis=0, tiled=True)]
  transfers between devices with their start and end apart: 7 -> 3, of which waited for: 7 -> 3; matrix products, arithmetic and copies ran while one was open for 11% -> 4% of each run, Pallas kernels for 0% -> 0%
where the time goes in v1:
time: 185 us; the launch traced here: 184 us
  Pallas kernels  122 us (66%)
  waiting for transfers between devices  20.9 us (11%)
  local copies, waits for them, and re-layouts  12.8 us (7%)
  starting transfers between devices  11.8 us (6%)
  matrix products  7.41 us (4%)
  other arithmetic  7.39 us (4%)
    pallas_call x1, Pallas kernels, moe(): pl.pallas_call(functools.partial(moe_kernel, (n_sp, n_x, n_z, pieces)), o...  122 us
    all_to_all x2, waiting for transfers between devices, sent_to_all(): return lax.all_to_all(copies, axis, split_axis=0, concat_axis=0, tiled=True)  14.6 us
    unnamed x68, local copies, waits for them, and re-layouts  8.9 us
    all_to_all x2, starting transfers between devices, sent_to_all(): return lax.all_to_all(copies, axis, split_axis=0, concat_axis=0, tiled=True)  8.07 us
    all_to_all x1, waiting for transfers between devices, local(): proj_all = lax.all_to_all(proj_part.astype(bf16), 'sp', 0, 0, tiled=True)  6.39 us
    all_to_all x1, starting transfers between devices, local(): proj_all = lax.all_to_all(proj_part.astype(bf16), 'sp', 0, 0, tiled=True)  3.72 us
  transfers between devices with their start and end apart: 3, of which 3 were waited for; matrix products, arithmetic and copies ran while one was open for 4% of the time, Pallas kernels for 0%

profile of v1, /device:TPU:96, one launch (start us, length us, event | category | flops | bytes accessed | tf_op | source)
XLA Modules:
  0.0 184.1 jit_solution(18426204355420224203)
XLA Ops:
  0.7 0.8 convert_negate_fusion
  1.5 0.1 copy.118
  1.7 0.1 fusion.9
  1.8 0.8 convert_multiply_fusion
  2.6 0.1 copy.117
  2.7 0.2 reduce_window_sum.33
  2.9 0.8 copy.115.ids
  3.7 0.8 copy.116.probs
  4.6 0.6 reshape.410.group
  5.1 122.1 %shard_map.188 = (f32[128,2048]{1,0:T(8,128)}, f32[128,2048]{1,0:T(8,128)}, f32[128,2048]{1,0:T(8,128)}, bf16[16,320,128]{2,1,0:T(8,128)(2,1)}, f32[320,128]{1,0:T(8,128)}) custom-call(bf16[320,128]{1,0:T(8,128)(2,1)} %layer_in.1, bf16[320,128]{1,0:T(8,128)(2,1)} %out_cot.1, s32[320,2]{1,0:T(8,128)} %copy.115.ids, f32[320,2]{1,0:T(8,128)} %copy.116.probs, ...), custom_call_target="tpu_custom_call" | custom-call | tf_op jit(solution)/shard_map/pallas_call | solution.py:489
  127.2 1.4 convolution_bitcast_fusion.1
  128.6 0.9 while.42
  128.7 0.1 bitcast_add_fusion.12
  128.8 0.1 bitcast_add_fusion.12
  129.6 0.8 broadcast_in_dim.120
  130.3 4.3 %all-to-all-start.2 = ((bf16[16,65,128]{2,1,0:T(8,128)(2,1)}), bf16[16,65,128]{2,1,0:T(8,128)(2,1)S(1)}, u32[]{:S(2)}, u32[]{:S(2)}) async-start(bf16[16,65,128]{2,1,0:T(8,128)(2,1)} %broadcast_in_dim.120), calls=%async_computation.2 | async-start | bytes 589824 | tf_op jit(solution)/shard_map/all_to_all | solution.py:539
  134.7 0.1 copy.119
  134.9 0.3 convolution_select_fusion
  135.1 0.4 convolution_select_fusion.1
  135.5 0.4 fusion.46
  136.0 0.2 fusion.45
  136.2 0.3 convolution_bitcast_fusion.2
  136.6 0.9 while.41
  137.5 0.4 copy-done.21
  138.0 0.4 convolution_multiply_fusion
  138.4 6.1 %all-to-all-done.2 = bf16[16,65,128]{2,1,0:T(8,128)(2,1)S(1)} async-done(((bf16[16,65,128]{2,1,0:T(8,128)(2,1)}), bf16[16,65,128]{2,1,0:T(8,128)(2,1)S(1)}, u32[]{:S(2)}, u32[]{:S(2)}) %all-to-all-start.2) | async-done | bytes 266272 | tf_op jit(solution)/shard_map/all_to_all | solution.py:539
  144.6 0.8 broadcast_in_dim.115
  145.3 3.7 %all-to-all-start = ((bf16[16,65,128]{2,1,0:T(8,128)(2,1)}), bf16[16,65,128]{2,1,0:T(8,128)(2,1)S(1)}, u32[]{:S(2)}, u32[]{:S(2)}) async-start(bf16[16,65,128]{2,1,0:T(8,128)(2,1)} %broadcast_in_dim.115), calls=%async_computation | async-start | bytes 589824 | tf_op jit(solution)/shard_map/all_to_all | solution.py:539
  149.3 8.4 %all-to-all-done = bf16[16,65,128]{2,1,0:T(8,128)(2,1)S(1)} async-done(((bf16[16,65,128]{2,1,0:T(8,128)(2,1)}), bf16[16,65,128]{2,1,0:T(8,128)(2,1)S(1)}, u32[]{:S(2)}, u32[]{:S(2)}) %all-to-all-start) | async-done | bytes 266272 | tf_op jit(solution)/shard_map/all_to_all | solution.py:539
  158.0 0.1 select_bitcast_fusion
  158.2 0.1 select_bitcast_fusion.1
  158.3 0.1 multiply_add_fusion.1
  158.5 0.1 multiply_add_fusion.3
  158.7 0.5 copy-done.6
  159.3 0.5 fusion.15
  159.7 0.3 fusion.6
  160.1 0.1 multiply_add_fusion
  160.2 0.1 multiply_add_fusion.2
  160.5 0.5 copy-done.8
  161.0 0.1 copy-done.11
  161.1 0.4 multiply_subtract_fusion
  161.5 0.1 copy.129
  161.6 0.2 reverse.4
  161.8 0.1 slice_bitcast_fusion.2
  162.0 0.9 reduce-window.6
  162.9 0.2 slice_reduce_fusion
  163.1 0.1 copy.140
  163.2 0.1 broadcast.153
  163.4 0.7 fusion.24
  164.0 0.4 fusion.7
  164.5 1.4 convolution_convert_fusion
  165.9 3.7 %all-to-all-start.1 = ((bf16[16,128,128]{2,1,0:T(8,128)(2,1)}), bf16[16,128,128]{2,1,0:T(8,128)(2,1)S(1)}, u32[]{:S(2)}, u32[]{:S(2)}) async-start(bf16[16,128,128]{2,1,0:T(8,128)(2,1)} %convolution_convert_fusion), calls=%async_computation.1 | async-start | bytes 1048576 | tf_op jit(solution)/shard_map/all_to_all | solution.py:703
  169.7 0.2 fusion.39
  169.9 0.2 reverse.5
  170.1 0.8 copy.133
  170.9 0.8 copy.134
  171.7 0.7 fusion.23
  172.4 1.0 convolution_add_fusion
  173.4 6.4 %all-to-all-done.1 = bf16[16,128,128]{2,1,0:T(8,128)(2,1)S(1)} async-done(((bf16[16,128,128]{2,1,0:T(8,128)(2,1)}), bf16[16,128,128]{2,1,0:T(8,128)(2,1)S(1)}, u32[]{:S(2)}, u32[]{:S(2)}) %all-to-all-start.1) | async-done | bytes 524320 | tf_op jit(solution)/shard_map/all_to_all | solution.py:703
  179.8 0.7 convert_reduce_fusion
  180.5 1.0 copy.205
  181.5 1.0 copy.206
  182.5 0.6 copy-done.3
  183.1 1.0 copy.207
  (158 shorter events, 2.5 us)
Async XLA Ops:
  0.6 134.2 %copy-start = (bf16[320,128]{1,0:T(8,128)(2,1)S(1)}, bf16[320,128]{1,0:T(8,128)(2,1)}, u32[]{:S(2)}) copy-start(bf16[320,128]{1,0:T(8,128)(2,1)} %param.28) | copy-start | bytes 245764
  0.6 2.3 %copy-start.25 = (s32[320,2]{0,1:T(2,128)S(1)}, s32[320,2]{0,1:T(2,128)}, u32[]{:S(2)}) copy-start(s32[320,2]{0,1:T(2,128)} %param.19) | copy-start | bytes 7684
  0.7 3.1 %copy-start.26 = (f32[320,2]{0,1:T(2,128)S(1)}, f32[320,2]{0,1:T(2,128)}, u32[]{:S(2)}) copy-start(f32[320,2]{0,1:T(2,128)} %param.20) | copy-start | bytes 7684
  0.7 3.9 %copy-start.27 = (f32[320]{0:T(512)S(1)}, f32[320]{0:T(512)}, u32[]{:S(2)}) copy-start(f32[320]{0:T(512)} %param.21) | copy-start | bytes 3844
  127.2 7.5 %copy-start.16 = (bf16[320,64]{0,1:T(8,128)(2,1)S(1)}, bf16[320,64]{0,1:T(8,128)(2,1)}, u32[]{:S(2)}) copy-start(bf16[320,64]{0,1:T(8,128)(2,1)} %param.27) | copy-start | bytes 122884
  128.6 6.3 %copy-start.1 = (f32[320,128]{1,0:T(8,128)S(1)}, f32[320,128]{1,0:T(8,128)}, u32[]{:S(2)}) copy-start(f32[320,128]{1,0:T(8,128)} %get-tuple-element.205) | copy-start | bytes 491524
  129.5 31.0 %copy-start.17 = (f32[5,1,64]{2,0,1:T(8,128)}, f32[5,1,64]{2,0,1:T(8,128)S(1)}, u32[]{:S(2)}) copy-start(f32[5,1,64]{2,0,1:T(8,128)S(1)} %get-tuple-element.206) | copy-start | bytes 3844
  130.3 14.2 %all-to-all-start.2 = ((bf16[16,65,128]{2,1,0:T(8,128)(2,1)}), bf16[16,65,128]{2,1,0:T(8,128)(2,1)S(1)}, u32[]{:S(2)}, u32[]{:S(2)}) async-start(bf16[16,65,128]{2,1,0:T(8,128)(2,1)} %broadcast_in_dim.120), calls=%async_computation.2 | async-start | bytes 589824 | tf_op jit(solution)/shard_map/all_to_all | solution.py:539
  136.2 24.3 %copy-start.14 = (f32[1,5,1,64]{3,1,2,0:T(8,128)}, f32[1,5,1,64]{3,1,2,0:T(8,128)S(1)}, u32[]{:S(2)}) copy-start(f32[1,5,1,64]{3,1,2,0:T(8,128)S(1)} %copy.165) | copy-start | bytes 3844
  137.5 0.5 copy-start.21
  137.5 21.2 %copy-start.19 = (f32[5,1,64]{2,0,1:T(8,128)}, f32[5,1,64]{2,0,1:T(8,128)S(1)}, u32[]{:S(2)}) copy-start(f32[5,1,64]{2,0,1:T(8,128)S(1)} %get-tuple-element.201) | copy-start | bytes 3844
  145.3 12.4 %all-to-all-start = ((bf16[16,65,128]{2,1,0:T(8,128)(2,1)}), bf16[16,65,128]{2,1,0:T(8,128)(2,1)S(1)}, u32[]{:S(2)}, u32[]{:S(2)}) async-start(bf16[16,65,128]{2,1,0:T(8,128)(2,1)} %broadcast_in_dim.115), calls=%async_computation | async-start | bytes 589824 | tf_op jit(solution)/shard_map/all_to_all | solution.py:539
  158.2 2.2 %copy-start.23 = (f32[64]{0:T(128)}, f32[64]{0:T(128)S(1)}, u32[]{:S(2)}) copy-start(f32[64]{0:T(128)S(1)} %get-tuple-element.407) | copy-start | bytes 772
  158.6 0.6 copy-start.6
  160.4 0.6 copy-start.8
  160.5 0.6 copy-start.11
  161.5 2.6 %copy-start.20 = (f32[5,1,64]{2,0,1:T(8,128)S(1)}, f32[5,1,64]{2,0,1:T(8,128)}, u32[]{:S(2)}) copy-start(f32[5,1,64]{2,0,1:T(8,128)} %copy-done.19) | copy-start | bytes 3844
  161.5 2.9 %copy-start.2 = (bf16[16,320,128]{2,1,0:T(8,128)(2,1)S(1)}, bf16[16,320,128]{2,1,0:T(8,128)(2,1)}, u32[]{:S(2)}) copy-start(bf16[16,320,128]{2,1,0:T(8,128)(2,1)} %get-tuple-element.200) | copy-start | bytes 3932164
  164.4 5.2 %copy-start.7 = (f32[2,1,64,128]{3,2,0,1:T(8,128)S(1)}, f32[2,1,64,128]{3,2,0,1:T(8,128)}, u32[]{:S(2)}) copy-start(f32[2,1,64,128]{3,2,0,1:T(8,128)} %copy-done.6) | copy-start | bytes 196612
  164.4 5.2 %copy-start.9 = (f32[2,1,64,128]{3,2,1,0:T(8,128)S(1)}, f32[2,1,64,128]{3,2,1,0:T(8,128)}, u32[]{:S(2)}) copy-start(f32[2,1,64,128]{3,2,1,0:T(8,128)} %copy-done.8) | copy-start | bytes 196612
  164.4 5.2 %copy-start.22 = (f32[1,64]{1,0:T(1,128)S(1)}, f32[1,64]{1,0:T(1,128)}, u32[]{:S(2)}) copy-start(f32[1,64]{1,0:T(1,128)} %copy-done.21) | copy-start | bytes 772
  164.5 5.2 %copy-start.24 = (f32[64]{0:T(128)S(1)}, f32[64]{0:T(128)}, u32[]{:S(2)}) copy-start(f32[64]{0:T(128)} %copy-done.23) | copy-start | bytes 772
  164.5 5.4 %copy-start.10 = (f32[1,384,64]{1,2,0:T(8,128)S(1)}, f32[1,384,64]{1,2,0:T(8,128)}, u32[]{:S(2)}) copy-start(f32[1,384,64]{1,2,0:T(8,128)} %fusion.24) | copy-start | bytes 294916
  165.9 5.8 %copy-start.13 = (bf16[320,64]{0,1:T(8,128)(2,1)S(1)}, bf16[320,64]{0,1:T(8,128)(2,1)}, u32[]{:S(2)}) copy-start(bf16[320,64]{0,1:T(8,128)(2,1)} %param.29) | copy-start | bytes 122884
  165.9 6.5 %copy-start.12 = (f32[64,128]{1,0:T(8,128)S(1)}, f32[64,128]{1,0:T(8,128)}, u32[]{:S(2)}) copy-start(f32[64,128]{1,0:T(8,128)} %copy-done.11) | copy-start | bytes 98308
  165.9 6.5 %copy-start.15 = (f32[1,5,1,64]{3,1,2,0:T(8,128)S(1)}, f32[1,5,1,64]{3,1,2,0:T(8,128)}, u32[]{:S(2)}) copy-start(f32[1,5,1,64]{3,1,2,0:T(8,128)} %copy-done.14) | copy-start | bytes 3844
  165.9 6.5 %copy-start.18 = (f32[5,1,64]{2,0,1:T(8,128)S(1)}, f32[5,1,64]{2,0,1:T(8,128)}, u32[]{:S(2)}) copy-start(f32[5,1,64]{2,0,1:T(8,128)} %copy-done.17) | copy-start | bytes 3844
  165.9 13.9 %all-to-all-start.1 = ((bf16[16,128,128]{2,1,0:T(8,128)(2,1)}), bf16[16,128,128]{2,1,0:T(8,128)(2,1)S(1)}, u32[]{:S(2)}, u32[]{:S(2)}) async-start(bf16[16,128,128]{2,1,0:T(8,128)(2,1)} %convolution_convert_fusion), calls=%async_computation.1 | async-start | bytes 1048576 | tf_op jit(solution)/shard_map/all_to_all | solution.py:703
  169.6 10.9 %copy-start.5 = (f32[128,2048]{1,0:T(8,128)S(1)}, f32[128,2048]{1,0:T(8,128)}, u32[]{:S(2)}) copy-start(f32[128,2048]{1,0:T(8,128)} %get-tuple-element.197) | copy-start | bytes 3145732
  173.4 8.1 %copy-start.4 = (f32[128,2048]{1,0:T(8,128)S(1)}, f32[128,2048]{1,0:T(8,128)}, u32[]{:S(2)}) copy-start(f32[128,2048]{1,0:T(8,128)} %get-tuple-element.198) | copy-start | bytes 3145732
  181.5 1.6 copy-start.3

commit v2 on v1

--- a/solution.py
+++ b/solution.py
@@ -9,11 +9,9 @@
 
 DK = 64
 DV = 128
-BLOCK = 64
 
 
 decay_temp = 16.0
-highest = lax.Precision.HIGHEST
 f32, bf16 = jnp.float32, jnp.bfloat16
 MESH = pl.DeviceIdType.MESH
 
@@ -24,6 +22,30 @@
 
 def dot_nn(a, b):
     return lax.dot_general(a, b, (((1,), (0,)), ((), ())), preferred_element_type=f32)
+
+
+def dot_tn(a, b):
+    return lax.dot_general(a, b, (((0,), (0,)), ((), ())), preferred_element_type=f32)
+
+
+def parts_of(x, n):
+    if x.dtype == bf16:
+        return [x]
+    found = []
+    for _ in range(n):
+        top = x.astype(bf16)
+        found.append(top)
+        x = x - top.astype(f32)
+    return found
+
+
+def fine(dot, a, b, n=2):
+    a, b = parts_of(a, n), parts_of(b, n)
+    terms = [dot(p, q) for i, p in enumerate(a) for j, q in enumerate(b) if i + j < n]
+    total = terms[-1]
+    for term in terms[-2::-1]:
+        total = total + term
+    return total
 
 
 def moe_kernel(
@@ -37,11 +59,34 @@
     up,
     down,
     out_w,
+    query,
+    key_in,
+    value,
+    logit,
     gate_g,
     up_g,
     down_g,
+    proj_g,
+    query_g,
+    key_g,
+    value_g,
+    logit_g,
     full_cot,
     mixer_cot,
+    q_dec,
+    k_back,
+    k_end,
+    cumul,
+    scores,
+    within,
+    mix_t,
+    span_out,
+    span_in,
+    entry,
+    fut_out,
+    fut_in,
+    pj_out,
+    pj_in,
     send,
     sel_t,
     rows,
@@ -71,6 +116,12 @@
     tkd_r,
     misc_s,
     misc_r,
+    fw_s,
+    fw_r,
+    bw_s,
+    bw_r,
+    pj_s,
+    pj_r,
 ):
     n_sp, n_x, n_z, pieces = sizes
     n_y = n_sp // n_x
@@ -112,12 +163,21 @@
     for dev in (partner, above, below):
         pl.semaphore_signal(barrier, inc=1, device_id=dev, device_id_type=MESH)
 
+    t_row = lax.broadcasted_iota(jnp.int32, (toks, toks), 0)
+    t_col = lax.broadcasted_iota(jnp.int32, (toks, toks), 1)
+    diagonal = t_row == t_col
+
+    def as_row(column):
+        return jnp.sum(jnp.where(diagonal, column, 0.0), axis=0, keepdims=True)
+
+    def as_column(row):
+        return jnp.sum(jnp.where(diagonal, row, 0.0), axis=1, keepdims=True)
+
     experts = lax.broadcasted_iota(jnp.int32, (toks, 128), 1)
-    id0, id1 = ids[:, 0:1], ids[:, 1:2]
+    id0 = as_column(ids[0:1, :].astype(f32)).astype(jnp.int32)
+    id1 = as_column(ids[1:2, :].astype(f32)).astype(jnp.int32)
     hit0, hit1 = experts == id0, experts == id1
     chosen = (jnp.where(hit0, 1.0, 0.0) + jnp.where(hit1, 1.0, 0.0)).astype(bf16)
-    t_row = lax.broadcasted_iota(jnp.int32, (toks, toks), 0)
-    t_col = lax.broadcasted_iota(jnp.int32, (toks, toks), 1)
     earlier = jnp.where(t_col < t_row, 1.0, 0.0).astype(bf16)
     count = dot_nn(earlier, chosen)
     pos0 = jnp.sum(jnp.where(hit0, count, 0.0), axis=1, keepdims=True)
@@ -133,12 +193,7 @@
     sel_t[...] = (
         jnp.where(slots == slot0, 1.0, 0.0) + jnp.where(slots == slot1, 1.0, 0.0)
     ).astype(bf16)
-    diagonal = t_row == t_col
-
-    def as_row(column):
-        return jnp.sum(jnp.where(diagonal, column, 0.0), axis=0, keepdims=True)
-
-    p0, p1 = as_row(probs[:, 0:1]), as_row(probs[:, 1:2])
+    p0, p1 = probs[0:1, :], probs[1:2, :]
     w0 = group[...] * p0 / (p0 + p1)
     w1 = group[...] * p1 / (p0 + p1)
     slot0_row, slot1_row = as_row(slot0.astype(f32)), as_row(slot1.astype(f32))
@@ -186,7 +241,7 @@
 
     last = (half - 1) * pieces
 
-    def ring(n_pieces, where, sems_s, sems_r, sems_ds, sems_dr, own_ready, compute):
+    def ring(n_pieces, where, sems_s, sems_r, sems_ds, sems_dr, own_ready, compute, beside):
         h_p = n_pieces // 2
         total = (half - 1) * n_pieces + h_p
 
@@ -206,6 +261,7 @@
             return carry
 
         lax.fori_loop(0, n_pieces, own, 0)
+        beside()
 
         def own_compute(p, carry):
             across(tp, p, p).wait_recv()
@@ -290,7 +346,54 @@
     def feats(b):
         return pl.ds(pl.multiple_of(b * 2 * cols, 2 * cols), 2 * cols)
 
-    pre[...] = jnp.zeros_like(pre)
+    causal = t_col <= t_row
+
+    def to_peers(copy_of):
+        def one(r, carry):
+            copy_of(r).start()
+            return carry
+
+        lax.fori_loop(1, n_sp, one, 0)
+
+    def span_copy(r):
+        return remote(span_out, span_in.at[sp], fw_s.at[r], fw_r.at[r], (there(r), tp))
+
+    def future_copy(r):
+        return remote(fut_out, fut_in.at[sp], bw_s.at[r], bw_r.at[r], (there(r), tp))
+
+    def attend():
+        log_decay = jax.nn.log_sigmoid(logit[...].astype(f32)) / decay_temp
+        upto = jnp.where(causal, 1.0, 0.0).astype(bf16)
+        cum = fine(dot_nn, upto, log_decay, 3)
+        total = cum[toks - 1 : toks, :]
+        cumul[...] = cum
+        k = key_in[...].astype(f32)
+        q_dec[...] = query[...].astype(f32) * DK ** (-0.5) * jnp.exp(cum)
+        k_back[...] = k * jnp.exp(-cum)
+        k_end[...] = k * jnp.exp(total - cum)
+        span_out[0:DK, :] = fine(dot_tn, k_end[...], value[...])
+        span_out[DK : 2 * DK, :] = jnp.exp(fine(dot_tn, log_decay, jnp.ones((toks, DV), bf16), 3))
+        to_peers(span_copy)
+        span_in[sp] = span_out[...]
+        found = jnp.where(causal, fine(dot_nt, q_dec[...], k_back[...]), 0.0)
+        scores[...] = found
+        within[...] = fine(dot_nn, found, value[...])
+        pre[...] = jnp.zeros_like(pre)
+
+    def enter():
+        def arrived(r, carry):
+            span_copy(r).wait_recv()
+            return carry
+
+        lax.fori_loop(1, n_sp, arrived, 0)
+
+        def pass_on(s, state):
+            return jnp.where(s < sp, span_in[s, DK : 2 * DK, :] * state + span_in[s, 0:DK, :], state)
+
+        entry[...] = lax.fori_loop(0, n_sp, pass_on, jnp.zeros((DK, DV), f32))
+        mixed_out = within[...] + fine(dot_nn, q_dec[...], entry[...])
+        mix_t[...] = mixed_out.T.astype(bf16)
+
 
     def expert_in(b, p):
         w_gu = jnp.concatenate([gate[:, feats(b)], up[:, feats(b)]], axis=0)
@@ -309,6 +412,7 @@
         agd_r,
         rows_ready,
         expert_in,
+        attend,
     )
 
     def middle(p, carry):
@@ -359,6 +463,7 @@
         return carry
 
     lax.fori_loop(0, h_p, first, 0)
+    enter()
 
     def gradients(b):
         x = jnp.concatenate([rows[2 * b, 0], rows[2 * b + 1, 0]], axis=1)
@@ -438,10 +543,37 @@
     tok_half = toks // 2
     mixer_cot[...] = jnp.zeros_like(mixer_cot)
 
+    wide = 2 * n_z // n_sp
+
+    def proj_copy(j):
+        return remote(
+            pj_out.at[j],
+            pj_in.at[sp, lax.rem(j, wide)],
+            pj_s.at[j],
+            pj_r.at[sp, lax.rem(j, wide)],
+            (j // wide, tp),
+        )
+
     def project(b, p):
         at = pl.ds(pl.multiple_of(p * tok_half, tok_half), tok_half)
         c = jnp.concatenate([full_cot[2 * b, at, :], full_cot[2 * b + 1, at, :]], axis=1)
         mixer_cot[at, :] += dot_nn(c, out_w[feats(b), :])
+
+        @pl.when(p == 1)
+        def _():
+            whole = jnp.concatenate([full_cot[2 * b], full_cot[2 * b + 1]], axis=1)
+            found = dot_nn(mix_t[...], whole).astype(bf16)
+            for i in range(2):
+                j = 2 * b + i
+                pj_out[j] = found[:, i * cols : (i + 1) * cols]
+
+                @pl.when(j // wide == sp)
+                def _():
+                    pj_in[sp, lax.rem(j, wide)] = pj_out[j]
+
+                @pl.when(j // wide != sp)
+                def _():
+                    proj_copy(j).start()
 
     drain_toks = ring(
         2,
@@ -452,11 +584,65 @@
         tkd_r,
         lambda p: None,
         project,
+        lambda: None,
     )
+
+    cot = mixer_cot[...]
+    fut = fine(dot_tn, q_dec[...], cot)
+    fut_out[...] = fut.astype(bf16)
+    to_peers(future_copy)
+    cot_values = jnp.where(causal, fine(dot_nt, cot, value[...]), 0.0)
+    cum = cumul[...]
+    q_grad = jnp.exp(cum) * (fine(dot_nt, cot, entry[...]) + fine(dot_nn, cot_values, k_back[...]))
+    query_g[...] = q_grad * DK ** (-0.5)
+    key_part = jnp.exp(-cum) * fine(dot_tn, cot_values, q_dec[...])
+    value_g[...] = fine(dot_tn, scores[...], cot)
+
+    def fut_arrived(r, carry):
+        future_copy(r).wait_recv()
+        return carry
+
+    lax.fori_loop(1, n_sp, fut_arrived, 0)
+
+    def pass_back(i, state):
+        s = n_sp - 1 - i
+        return jnp.where(
+            s > sp, span_in[s, DK : 2 * DK, :] * state + fut_in[s].astype(f32), state
+        )
+
+    future = lax.fori_loop(0, n_sp, pass_back, jnp.zeros((DK, DV), f32))
+    k_grad = key_part + jnp.exp(cum[toks - 1 : toks, :] - cum) * fine(dot_nt, value[...], future)
+    key_g[...] = k_grad
+    value_g[...] += fine(dot_nn, k_end[...], future)
+    span_end = span_out[DK : 2 * DK, :] * entry[...] + span_out[0:DK, :]
+    beyond = fine(dot_nt, jnp.ones((8, DV), bf16), future * span_end, 3)[0:1, :]
+    terms = query[...].astype(f32) * DK ** (-0.5) * q_grad - key_in[...].astype(f32) * k_grad
+    since = jnp.where(t_col >= t_row, 1.0, 0.0).astype(bf16)
+    tail = fine(dot_nn, since, terms, 3) + beyond
+    logit_g[...] = tail * jax.nn.sigmoid(-logit[...].astype(f32)) / decay_temp
+
+    def proj_arrived(s, carry):
+        for i in range(wide):
+            @pl.when(s != sp)
+            def _():
+                remote(
+                    pj_out.at[0], pj_in.at[s, i], pj_s.at[0], pj_r.at[s, i], (sp, tp)
+                ).wait_recv()
+
+        return carry
+
+    lax.fori_loop(0, n_sp, proj_arrived, 0)
+    for i in range(wide):
+        sums = jnp.zeros((128, cols), f32)
+        for s in range(n_sp):
+            sums = sums + pj_in[s, i].astype(f32)
+        proj_g[i * cols : (i + 1) * cols, :] = sums.T
 
     def sent(r, carry):
         dispatch(r).wait_send()
         give_back(r).wait_send()
+        span_copy(r).wait_send()
+        future_copy(r).wait_send()
         return carry
 
     lax.fori_loop(1, n_sp, sent, 0)
@@ -469,35 +655,79 @@
         return carry
 
     lax.fori_loop(0, rs_total, sums_sent, 0)
+
+    def proj_sent(j, carry):
+        @pl.when(j // wide != sp)
+        def _():
+            proj_copy(j).wait_send()
+
+        return carry
+
+    lax.fori_loop(0, 2 * n_z, proj_sent, 0)
     drain_rows()
     drain_toks()
 
 
-def moe(layer_in, out_cot, ids, probs, group, gate, up, down, out_w, n_sp, n_tp):
+def local(
+    layer_in,
+    out_cot,
+    route_ids,
+    route_probs,
+    group_prob,
+    gate_weight,
+    up_weight,
+    down_weight,
+    out_weight,
+    query,
+    key_in,
+    value,
+    decay_logit,
+):
     toks, cols = layer_in.shape
+    n_sp, n_tp = lax.axis_size("sp"), lax.axis_size("tp")
     n_x = 4 if n_sp == 16 else n_sp
     n_z = n_tp // 2
     half = n_z // 2
     pieces = 4 if n_sp % 4 == 0 else 2
-    width = gate.shape[1]
+    width = gate_weight.shape[2]
     n_rows = 4 * toks
     total = (half - 1) * pieces + pieces // 2
     tk_total = (half - 1) * 2 + 1
     chunk = n_rows // pieces
+    wide = n_tp // n_sp
     dma = pltpu.SemaphoreType.DMA
     vmem = pl.BlockSpec(memory_space=pltpu.VMEM)
-    return pl.pallas_call(
+    gate_g, up_g, down_g, *rest = pl.pallas_call(
         functools.partial(moe_kernel, (n_sp, n_x, n_z, pieces)),
         out_shape=(
             jax.ShapeDtypeStruct((128, width), f32),
             jax.ShapeDtypeStruct((128, width), f32),
             jax.ShapeDtypeStruct((128, width), f32),
-            jax.ShapeDtypeStruct((n_tp, toks, cols), bf16),
-            jax.ShapeDtypeStruct((toks, 128), f32),
+            jax.ShapeDtypeStruct((wide * cols, DV), f32),
+            jax.ShapeDtypeStruct((toks, DK), f32),
+            jax.ShapeDtypeStruct((toks, DK), f32),
+            jax.ShapeDtypeStruct((toks, DV), f32),
+            jax.ShapeDtypeStruct((toks, DK), f32),
         ),
-        in_specs=[vmem] * 9,
-        out_specs=[vmem] * 5,
+        in_specs=[vmem] * 13,
+        out_specs=[vmem] * 8,
         scratch_shapes=[
+            pltpu.VMEM((n_tp, toks, cols), bf16),
+            pltpu.VMEM((toks, DV), f32),
+            pltpu.VMEM((toks, DK), f32),
+            pltpu.VMEM((toks, DK), f32),
+            pltpu.VMEM((toks, DK), f32),
+            pltpu.VMEM((toks, DK), f32),
+            pltpu.VMEM((toks, toks), f32),
+            pltpu.VMEM((toks, DV), f32),
+            pltpu.VMEM((DV, toks), bf16),
+            pltpu.VMEM((2 * DK, DV), f32),
+            pltpu.VMEM((n_sp, 2 * DK, DV), f32),
+            pltpu.VMEM((DK, DV), f32),
+            pltpu.VMEM((DK, DV), bf16),
+            pltpu.VMEM((n_sp, DK, DV), bf16),
+            pltpu.VMEM((n_tp, DV, cols), bf16),
+            pltpu.VMEM((n_sp, wide, DV, cols), bf16),
             pltpu.VMEM((2, n_rows, cols), bf16),
             pltpu.VMEM((toks, n_rows), bf16),
             pltpu.VMEM((n_tp, 2, n_rows, cols), bf16),
@@ -527,235 +757,32 @@
             dma((2 + 2 * tk_total,)),
             dma((3,)),
             dma((3,)),
+            dma((n_sp,)),
+            dma((n_sp,)),
+            dma((n_sp,)),
+            dma((n_sp,)),
+            dma((n_tp,)),
+            dma((n_sp, wide)),
         ],
         compiler_params=pltpu.CompilerParams(
             collective_id=0, has_side_effects=True, vmem_limit_bytes=60 * 1024 * 1024
         ),
-    )(layer_in, out_cot, ids, probs, group, gate, up, down, out_w)
-
-
-def sent_to_all(x, axis):
-    copies = jnp.broadcast_to(x, (lax.axis_size(axis), *x.shape))
-    return lax.all_to_all(copies, axis, split_axis=0, concat_axis=0, tiled=True)
-
-
-def all_in_one(x, axis):
-    leaves = jax.tree.leaves(x)
-    turns = sorted(range(len(leaves)), key=lambda k: -leaves[k].size)
-    width = (1, *leaves[turns[0]].shape)[-1]
-    lines = [
-        jnp.pad(leaves[k].reshape(-1), (0, -leaves[k].size % width)).reshape(-1, width)
-        for k in turns
-    ]
-    both, at, found = (sent_to_all(jnp.concatenate(lines), axis), 0, {})
-    for k, line in zip(turns, lines):
-        section = both[:, at : at + len(line)].reshape(len(both), -1)
-        found[k] = section[:, : leaves[k].size].reshape(-1, *leaves[k].shape)
-        at += len(line)
-    numbers = iter(range(len(leaves)))
-    return jax.tree.map(lambda _: found[next(numbers)], x)
-
-
-def folded_in_pairs(pieces, combine):
-    while len(jax.tree.leaves(pieces)[0]) > 1:
-        pieces = jax.vmap(combine)(
-            *(jax.tree.map(lambda part: part[side::2], pieces) for side in (0, 1))
-        )
-    return jax.tree.map(lambda part: part[0], pieces)
-
-
-def entering(x, axis, combine, identity, reverse):
-    length, index = (lax.axis_size(axis), lax.axis_index(axis))
-    passed = jnp.arange(length) > index if reverse else jnp.arange(length) < index
-
-    def kept(part, zero, own):
-        part = jnp.where(
-            passed.reshape(-1, *(1 for _ in own.shape)),
-            part.astype(own.dtype),
-            jnp.asarray(zero, own.dtype),
-        )
-        return part[::-1] if reverse else part
-
-    pieces = all_in_one(
-        jax.tree.map(
-            lambda part, kind: part.astype(kind),
-            x,
-            jax.tree.map(lambda a: jnp.bfloat16 if a.dtype == jnp.float32 else a.dtype, x),
-        ),
-        axis,
-    )
-    return folded_in_pairs(jax.tree.map(kept, pieces, identity, x), combine)
-
-
-def in_blocks(x, dim, length):
-    lengths = x.shape
-    blocks = x.reshape(*lengths[:dim], length, lengths[dim] // length, *lengths[dim + 1 :])
-    return jnp.moveaxis(blocks, dim, 0)
-
-
-def summed_on_arrival(x, axis, dim):
-    length = lax.axis_size(axis)
-    blocks = lax.all_to_all(in_blocks(x, dim, length), axis, 0, 0, tiled=True)
-    return jnp.sum(blocks.astype(jnp.float32), axis=0)
-
-
-def combine_spans(earlier, later):
-    return (earlier[0] * later[0], later[1] + later[0][..., None] * earlier[1])
-
-
-def contract_rows(left_mat, right_mat):
-    return lax.dot_general(
-        left_mat, right_mat, (((0,), (0,)), ((), ())), preferred_element_type=jnp.float32
-    )
-
-
-def contract_cols(left_mat, right_mat):
-    return lax.dot_general(
-        left_mat, right_mat, (((1,), (1,)), ((), ())), preferred_element_type=jnp.float32
-    )
-
-
-def to_blocks(tensor, head_count):
-    rows_here = tensor.shape[0]
-    return (
-        tensor.astype(jnp.float32)
-        .reshape(rows_here // BLOCK, BLOCK, head_count, -1)
-        .transpose(2, 0, 1, 3)
-    )
-
-
-def from_blocks(tensor):
-    head_count, blocks, _, channels = tensor.shape
-    return tensor.transpose(1, 2, 0, 3).reshape(blocks * BLOCK, head_count * channels)
-
-
-def local(
-    layer_in,
-    out_cot,
-    route_ids,
-    route_probs,
-    group_prob,
-    gate_weight,
-    up_weight,
-    down_weight,
-    out_weight,
-    query,
-    key_in,
-    value,
-    decay_logit,
-):
-    tok_rows = layer_in.shape[0]
-    head_dev = query.shape[1] // DK
-    scaled_query = to_blocks(query, head_dev) * DK ** (-0.5)
-    key_blk = to_blocks(key_in, head_dev)
-    value_blk = to_blocks(value, head_dev)
-    logit_blk = to_blocks(decay_logit, head_dev)
-    cumulative = jnp.cumsum(jax.nn.log_sigmoid(logit_blk) / decay_temp, axis=2)
-    span_log = cumulative[:, :, -1:, :]
-    growth = jnp.exp(cumulative)
-    shrink = jnp.exp(-cumulative)
-    to_end = jnp.exp(span_log - cumulative)
-    query_decayed = scaled_query * growth
-    key_back = key_blk * shrink
-    key_to_end = key_blk * to_end
-    causal = jnp.tril(jnp.ones((BLOCK, BLOCK), dtype=bool))
-    scores = jnp.where(
-        causal, jnp.einsum("hncd,hnsd->hncs", query_decayed, key_back, precision=highest), 0.0
-    )
-    within = jnp.einsum("hncs,hnsv->hncv", scores, value_blk, precision=highest)
-    block_decay = jnp.moveaxis(jnp.exp(span_log[:, :, 0, :]), 1, 0)
-    block_update = jnp.moveaxis(
-        jnp.einsum("hncd,hncv->hndv", key_to_end, value_blk, precision=highest), 1, 0
-    )
-    identity_pair = (
-        jnp.ones((head_dev, DK), jnp.float32),
-        jnp.zeros((head_dev, DK, DV), jnp.float32),
-    )
-
-    def advance(carry_pair, inputs):
-        return (combine_spans(carry_pair, inputs), carry_pair)
-
-    span_total, before_pairs = lax.scan(advance, identity_pair, (block_decay, block_update))
-    entry_pair = entering(span_total, "sp", combine_spans, identity_pair, False)
-    entry_state = entry_pair[1]
-    decay_before = jnp.moveaxis(before_pairs[0], 0, 1)
-    block_state = decay_before[..., None] * entry_state[:, None] + jnp.moveaxis(
-        before_pairs[1], 0, 1
-    )
-    span_end = span_total[0][..., None] * entry_state + span_total[1]
-    outputs = within + jnp.einsum("hncd,hndv->hncv", query_decayed, block_state, precision=highest)
-    mixer_out = from_blocks(outputs).astype(jnp.bfloat16)
-    n_sp, n_tp = lax.axis_size("sp"), lax.axis_size("tp")
-    gate_g, up_g, down_g, full_cot, mixer_cot = moe(
+    )(
         layer_in,
         out_cot,
-        route_ids,
-        route_probs,
-        group_prob.reshape(1, tok_rows),
+        route_ids.T,
+        route_probs.T,
+        group_prob.reshape(1, toks),
         gate_weight[0],
         up_weight[0],
         down_weight[0],
         out_weight,
-        n_sp,
-        n_tp,
+        query,
+        key_in,
+        value,
+        decay_logit,
     )
-    proj_part = jnp.einsum("btf,tv->bfv", full_cot, mixer_out, preferred_element_type=f32)
-    proj_all = lax.all_to_all(proj_part.astype(bf16), "sp", 0, 0, tiled=True)
-    proj_grad = jnp.sum(proj_all.astype(f32), axis=0)
-    cot_blk = to_blocks(mixer_cot, head_dev)
-    block_future = jnp.moveaxis(
-        jnp.einsum("hncd,hncv->hndv", query_decayed, cot_blk, precision=highest), 1, 0
-    )
-
-    def retreat(carry_pair, inputs):
-        return (combine_spans(carry_pair, inputs), carry_pair)
-
-    span_back, after_pairs = lax.scan(
-        retreat, identity_pair, (block_decay, block_future), reverse=True
-    )
-    beyond_pair = entering(span_back, "sp", combine_spans, identity_pair, True)
-    future_state = beyond_pair[1]
-    decay_after = jnp.moveaxis(after_pairs[0], 0, 1)
-    block_future_state = decay_after[..., None] * future_state[:, None] + jnp.moveaxis(
-        after_pairs[1], 0, 1
-    )
-    cot_values = jnp.where(
-        causal, jnp.einsum("hncv,hnsv->hncs", cot_blk, value_blk, precision=highest), 0.0
-    )
-    query_scaled_grad = growth * (
-        jnp.einsum("hncv,hndv->hncd", cot_blk, block_state, precision=highest)
-        + jnp.einsum("hncs,hnsd->hncd", cot_values, key_back, precision=highest)
-    )
-    key_part = shrink * jnp.einsum("hncs,hncd->hnsd", cot_values, query_decayed, precision=highest)
-    key_grad = key_part + to_end * jnp.einsum(
-        "hnsv,hndv->hnsd", value_blk, block_future_state, precision=highest
-    )
-    value_grad = jnp.einsum("hncs,hncv->hnsv", scores, cot_blk, precision=highest) + jnp.einsum(
-        "hnsd,hndv->hnsv", key_to_end, block_future_state, precision=highest
-    )
-    decay_terms = (scaled_query * query_scaled_grad - key_blk * key_grad).reshape(
-        head_dev, tok_rows, DK
-    )
-    tail_sum = jnp.flip(jnp.cumsum(jnp.flip(decay_terms, 1), axis=1), 1)
-    beyond_term = jnp.sum(future_state * span_end, axis=2)
-    log_grad = tail_sum + beyond_term[:, None, :]
-    logit_flat = logit_blk.reshape(head_dev, tok_rows, DK)
-    logit_grad = (
-        (log_grad * jax.nn.sigmoid(-logit_flat) / decay_temp)
-        .transpose(1, 0, 2)
-        .reshape(tok_rows, head_dev * DK)
-    )
-    query_grad = from_blocks(query_scaled_grad * DK ** (-0.5))
-    return (
-        gate_g[None],
-        up_g[None],
-        down_g[None],
-        proj_grad,
-        query_grad,
-        from_blocks(key_grad),
-        from_blocks(value_grad),
-        logit_grad,
-    )
+    return (gate_g[None], up_g[None], down_g[None], *rest)
 
 
 def solution(mesh):

time: 185 us -> 150 us (0.81)
  waiting for transfers between devices: 20.9 us -> 0 us
  starting transfers between devices: 11.8 us -> 0 us
  Pallas kernels: 122 us -> 133 us
  matrix products: 7.41 us -> 0 us
  other arithmetic: 7.39 us -> 0 us
    all_to_all x3 -> x0, waiting for transfers between devices: 20.9 us -> none  [the longest x2 14.6 us: sent_to_all(): return lax.all_to_all(copies, axis, split_axis=0, concat_axis=0, tiled=True)]
    all_to_all x3 -> x0, starting transfers between devices: 11.8 us -> none  [the longest x2 8.07 us: sent_to_all(): return lax.all_to_all(copies, axis, split_axis=0, concat_axis=0, tiled=True)]
    pallas_call x1, Pallas kernels: 122 us -> 133 us  [local(): pl.pallas_call(functools.partial(moe_kernel, (n_sp, n_x, n_z, pieces)), o...]
    dot_general x13 -> x0, matrix products: 7.41 us -> none  [the longest x1 1.43 us: local(): jnp.einsum('btf,tv->bfv', full_cot, mixer_out, preferred_element_type=f32)]
    unnamed x68 -> x29, local copies, waits for them, and re-layouts: 8.9 us -> 13.4 us
    another operation x5 -> x0, other arithmetic: 2.48 us -> none
  transfers between devices with their start and end apart: 3 -> 0, of which waited for: 3 -> 0; matrix products, arithmetic and copies ran while one was open for 4% -> 0% of each run, Pallas kernels for 0% -> 0%
where the time goes in v2:
time: 150 us; the launch traced here: 148 us
  Pallas kernels  133 us (89%)
  local copies, waits for them, and re-layouts  14 us (9%)
    pallas_call x1, Pallas kernels, local(): pl.pallas_call(functools.partial(moe_kernel, (n_sp, n_x, n_z, pieces)), o...  133 us
    unnamed x29, local copies, waits for them, and re-layouts  13.4 us

profile of v2, /device:TPU:96, one launch (start us, length us, event | category | flops | bytes accessed | tf_op | source)
XLA Modules:
  0.0 148.0 jit_solution(12363732500545709607)
XLA Ops:
  0.6 0.0 copy-start.8
  0.6 0.7 copy-done.8
  1.3 0.6 reshape.19.group
  1.9 0.0 copy-start.6
  1.9 1.5 %copy.21.query = bf16[320,64]{1,0:T(8,128)(2,1)} copy(bf16[320,64]{0,1:T(8,128)(2,1)} %param.22) | data formatting | bytes 81920 | tf_op args[9]
  3.4 0.0 copy-done.6
  3.4 0.0 copy-start.7
  3.4 0.7 copy.22.key_in
  4.2 0.1 copy-done.7
  4.2 0.7 copy.23.logit
  5.0 133.3 %shard_map.188 = (f32[128,2048]{1,0:T(8,128)}, f32[128,2048]{1,0:T(8,128)}, f32[128,2048]{1,0:T(8,128)}, f32[128,128]{1,0:T(8,128)}, f32[320,64]{1,0:T(8,128)}, ...) custom-call(bf16[320,128]{1,0:T(8,128)(2,1)} %layer_in.1, bf16[320,128]{1,0:T(8,128)(2,1)} %out_cot.1, ...), custom_call_target="tpu_custom_call" | custom-call | tf_op jit(solution)/shard_map/pallas_call | solution.py:700
  138.3 0.0 copy-start.4
  138.3 1.7 %copy.24 = f32[320,64]{0,1:T(8,128)} copy(f32[320,64]{1,0:T(8,128)} %get-tuple-element.28) | data formatting | bytes 163840
  140.0 0.0 copy-done.4
  140.0 0.0 copy-start.3
  140.0 0.8 copy.25
  140.8 0.2 copy-done.3
  140.9 0.8 copy.26
  141.7 0.0 copy-start.1
  141.7 2.4 %copy.32 = f32[1,128,2048]{2,1,0:T(8,128)} copy(f32[1,128,2048]{2,1,0:T(8,128)} %bitcast.10) | data formatting | bytes 2097152
  144.1 0.0 copy-done.1
  144.1 0.0 copy-start
  144.1 1.0 copy.33
  145.1 0.6 copy-done
  145.7 0.0 copy-start.5
  145.7 0.0 copy-start.2
  145.7 1.0 copy.34
  146.7 0.0 copy-done.5
  146.7 0.6 copy.35
  147.3 0.0 copy-done.2
  147.3 0.7 copy.36
Async XLA Ops:
  0.6 0.7 copy-start.8
  1.9 1.5 %copy-start.6 = (bf16[320,64]{0,1:T(8,128)(2,1)S(1)}, bf16[320,64]{0,1:T(8,128)(2,1)}, u32[]{:S(2)}) copy-start(bf16[320,64]{0,1:T(8,128)(2,1)} %param.23) | copy-start | bytes 122884
  3.4 0.8 copy-start.7
  138.3 1.7 %copy-start.4 = (f32[320,64]{1,0:T(8,128)S(1)}, f32[320,64]{1,0:T(8,128)}, u32[]{:S(2)}) copy-start(f32[320,64]{1,0:T(8,128)} %get-tuple-element.29) | copy-start | bytes 245764
  140.0 0.9 copy-start.3
  141.7 2.4 %copy-start.1 = (f32[128,2048]{1,0:T(8,128)S(1)}, f32[128,2048]{1,0:T(8,128)}, u32[]{:S(2)}) copy-start(f32[128,2048]{1,0:T(8,128)} %get-tuple-element.17) | copy-start | bytes 3145732
  144.1 1.6 %copy-start = (f32[128,2048]{1,0:T(8,128)S(1)}, f32[128,2048]{1,0:T(8,128)}, u32[]{:S(2)}) copy-start(f32[128,2048]{1,0:T(8,128)} %get-tuple-element.18) | copy-start | bytes 3145732
  145.7 1.0 copy-start.5
  145.7 1.6 %copy-start.2 = (f32[320,128]{1,0:T(8,128)S(1)}, f32[320,128]{1,0:T(8,128)}, u32[]{:S(2)}) copy-start(f32[320,128]{1,0:T(8,128)} %get-tuple-element.46) | copy-start | bytes 491524

commit v3 on v2

--- a/solution.py
+++ b/solution.py
@@ -50,11 +50,24 @@
 
 def moe_kernel(
     sizes,
-    layer_in,
-    out_cot,
     ids,
     probs,
     group,
+    *refs,
+):
+    held, given, kept = refs[:10], refs[10:18], refs[18:]
+    expert_kernel(sizes, ids, probs, group, held, given, *kept)
+
+
+def expert_kernel(
+    sizes,
+    ids,
+    probs,
+    group,
+    held,
+    given,
+    layer_in,
+    out_cot,
     gate,
     up,
     down,
@@ -116,16 +129,32 @@
     tkd_r,
     misc_s,
     misc_r,
+    gu_s,
+    gu_r,
     fw_s,
     fw_r,
     bw_s,
     bw_r,
     pj_s,
     pj_r,
+    load_s,
+    give_s,
 ):
     n_sp, n_x, n_z, pieces = sizes
     n_y = n_sp // n_x
     half = n_z // 2
+    targets = (layer_in, out_cot, gate, up, down, out_w, query, key_in, value, logit)
+    loaded = [
+        pltpu.make_async_copy(source, target, load_s.at[k])
+        for k, (source, target) in enumerate(zip(held, targets))
+    ]
+    for k in (0, 1, 2, 3, 6, 7, 8, 9, 4, 5):
+        loaded[k].start()
+    results = (gate_g, up_g, down_g, proj_g, query_g, key_g, value_g, logit_g)
+    stored = [
+        pltpu.make_async_copy(source, target, give_s.at[k])
+        for k, (source, target) in enumerate(zip(results, given))
+    ]
     toks, cols = layer_in.shape
     cap = 4 * toks // n_sp
     n_rows = n_sp * cap
@@ -194,9 +223,12 @@
         jnp.where(slots == slot0, 1.0, 0.0) + jnp.where(slots == slot1, 1.0, 0.0)
     ).astype(bf16)
     p0, p1 = probs[0:1, :], probs[1:2, :]
-    w0 = group[...] * p0 / (p0 + p1)
-    w1 = group[...] * p1 / (p0 + p1)
+    group_row = group[...].reshape(1, toks)
+    w0 = group_row * p0 / (p0 + p1)
+    w1 = group_row * p1 / (p0 + p1)
     slot0_row, slot1_row = as_row(slot0.astype(f32)), as_row(slot1.astype(f32))
+    loaded[0].wait()
+    loaded[1].wait()
     both = jnp.concatenate([layer_in[...], out_cot[...]], axis=1)
 
     def select(p, carry):
@@ -217,6 +249,8 @@
         remote(w, part_w.at[k], misc_s.at[k], misc_r.at[k], partner)
         for k, w in enumerate((gate, up))
     ]
+    loaded[2].wait()
+    loaded[3].wait()
     for copy in give_w:
         copy.start()
 
@@ -227,8 +261,8 @@
         return remote(
             send.at[:, slot_rows(r), :],
             rows.at[tp, :, slot_rows(r), :],
-            a2a_s.at[r],
-            a2a_r.at[r],
+            a2a_s,
+            a2a_r.at[r // per],
             (there(r), tp),
         )
 
@@ -247,11 +281,11 @@
 
         def along(block, p, d, k):
             ref = where(block, p)
-            return remote(ref, ref, sems_s.at[d, k], sems_r.at[d, k], above if d == 0 else below)
+            return remote(ref, ref, sems_s, sems_r.at[d, k], above if d == 0 else below)
 
         def across(block, p, k):
             ref = where(block, p)
-            return remote(ref, ref, sems_ds.at[k], sems_dr.at[k], partner)
+            return remote(ref, ref, sems_ds, sems_dr.at[k], partner)
 
         def own(p, carry):
             own_ready(p)
@@ -316,32 +350,20 @@
         lax.fori_loop(0, total, step, 0)
         use(total - 1)
 
-        def drain():
-            def one(k, carry):
-                along(tp, 0, 0, k).wait_send()
-                along(tp, 0, 1, k).wait_send()
-                return carry
-
-            lax.fori_loop(0, total, one, 0)
-
-            def other(k, carry):
-                across(tp, 0, k).wait_send()
-                return carry
-
-            lax.fori_loop(0, n_pieces + 2 * total, other, 0)
-
-        return drain
 
     def piece_rows(p):
         return pl.ds(pl.multiple_of(p * chunk, chunk), chunk)
 
     def rows_ready(p):
-        for i in range(per):
-            r = p * per + i
-
-            @pl.when(r > 0)
-            def _():
-                dispatch(r).wait_recv()
+        @pl.when((p == 0) & (per > 1))
+        def _():
+            came = rows.at[tp, :, cap:chunk, :]
+            remote(came, came, a2a_s, a2a_r.at[0], partner).wait_recv()
+
+        @pl.when(p > 0)
+        def _():
+            came = rows.at[tp, :, piece_rows(p), :]
+            remote(came, came, a2a_s, a2a_r.at[p], partner).wait_recv()
 
     def feats(b):
         return pl.ds(pl.multiple_of(b * 2 * cols, 2 * cols), 2 * cols)
@@ -356,19 +378,28 @@
         lax.fori_loop(1, n_sp, one, 0)
 
     def span_copy(r):
-        return remote(span_out, span_in.at[sp], fw_s.at[r], fw_r.at[r], (there(r), tp))
+        return remote(span_out, span_in.at[sp], fw_s, fw_r, (there(r), tp))
 
     def future_copy(r):
-        return remote(fut_out, fut_in.at[sp], bw_s.at[r], bw_r.at[r], (there(r), tp))
+        return remote(fut_out, fut_in.at[sp], bw_s.at[r], bw_r.at[sp], (there(r), tp))
+
+    def to_earlier(r, carry):
+        @pl.when(there(r) < sp)
+        def _():
+            future_copy(r).start()
+
+        return carry
 
     def attend():
-        log_decay = jax.nn.log_sigmoid(logit[...].astype(f32)) / decay_temp
+        for k in (6, 7, 8, 9, 4, 5):
+            loaded[k].wait()
+        log_decay = jax.nn.log_sigmoid(logit[...].astype(f32).T) / decay_temp
         upto = jnp.where(causal, 1.0, 0.0).astype(bf16)
         cum = fine(dot_nn, upto, log_decay, 3)
         total = cum[toks - 1 : toks, :]
         cumul[...] = cum
-        k = key_in[...].astype(f32)
-        q_dec[...] = query[...].astype(f32) * DK ** (-0.5) * jnp.exp(cum)
+        k = key_in[...].astype(f32).T
+        q_dec[...] = query[...].astype(f32).T * DK ** (-0.5) * jnp.exp(cum)
         k_back[...] = k * jnp.exp(-cum)
         k_end[...] = k * jnp.exp(total - cum)
         span_out[0:DK, :] = fine(dot_tn, k_end[...], value[...])
@@ -381,11 +412,8 @@
         pre[...] = jnp.zeros_like(pre)
 
     def enter():
-        def arrived(r, carry):
-            span_copy(r).wait_recv()
-            return carry
-
-        lax.fori_loop(1, n_sp, arrived, 0)
+        came = span_in.at[1:]
+        remote(came, came, fw_s, fw_r, partner).wait_recv()
 
         def pass_on(s, state):
             return jnp.where(s < sp, span_in[s, DK : 2 * DK, :] * state + span_in[s, 0:DK, :], state)
@@ -403,7 +431,7 @@
         pre[at, 0:256] += dot_nt(x, w_gu)
         pre[at, 256:384] += dot_nt(c, down[:, feats(b)])
 
-    drain_rows = ring(
+    ring(
         pieces,
         lambda block, p: rows.at[block, :, piece_rows(p), :],
         ag_s,
@@ -415,29 +443,28 @@
         attend,
     )
 
-    def middle(p, carry):
+    h_p = pieces // 2
+
+    def give_gu(p):
+        at = piece_rows(p)
+        return remote(gu.at[at, :], gu_part.at[at, :], gu_s, gu_r.at[p], partner)
+
+    def middle(i, carry):
+        p = i // 2 + lax.rem(i, 2) * h_p
         at = piece_rows(p)
         gate_pre, up_pre, hidden_cot = pre[at, 0:128], pre[at, 128:256], pre[at, 256:384]
         sig = jax.nn.sigmoid(gate_pre)
         active = gate_pre * sig
-        hidden = active * up_pre
-        up_cot = (hidden_cot * active).astype(bf16)
-        gate_cot = (hidden_cot * up_pre * sig * (1.0 + gate_pre * (1.0 - sig))).astype(bf16)
-        gu[at, 0:128] = gate_cot
-        gu[at, 128:256] = up_cot
-        pre[at, 0:128] = hidden
+        gu[at, 0:128] = (hidden_cot * up_pre * sig * (1.0 + gate_pre * (1.0 - sig))).astype(bf16)
+        gu[at, 128:256] = (hidden_cot * active).astype(bf16)
+        give_gu(p).start()
+        pre[at, 0:128] = active * up_pre
         return carry
 
     lax.fori_loop(0, pieces, middle, 0)
-    give_gu = remote(gu, gu_part, misc_s.at[2], misc_r.at[2], partner)
-    give_gu.start()
-    gu_t[...] = gu[...].T
-    hid_t[...] = pre[:, 0:128].astype(bf16).T
     for copy in give_w:
         copy.wait_recv()
-    give_gu.wait_recv()
-
-    h_p = pieces // 2
+
     rs_total = h_p + (half - 1) * pieces
 
     def partial(b, p):
@@ -451,18 +478,21 @@
         return remote(
             stage.at[d, k],
             inbox.at[d, k],
-            rs_s.at[d, k],
+            rs_s,
             rs_r.at[d, k],
             above if d == 0 else below,
         )
 
     def first(t, carry):
         for d in range(2):
+            give_gu(t + d * h_p).wait_recv()
             stage[d, t] = partial(zpos(half), t + d * h_p).astype(bf16)
             hop_sum(d, t).start()
         return carry
 
     lax.fori_loop(0, h_p, first, 0)
+    gu_t[...] = gu[...].T
+    hid_t[...] = pre[:, 0:128].astype(bf16).T
     enter()
 
     def gradients(b):
@@ -506,8 +536,8 @@
         return remote(
             ret_out.at[slot_rows(r), :],
             ret.at[slot_rows(r), :],
-            back_s.at[r],
-            back_r.at[r],
+            back_s,
+            back_r,
             (back_to(r), tp),
         )
 
@@ -530,13 +560,12 @@
     lax.fori_loop(0, pieces, finish, 0)
     for g in range(rs_total - h_p, n_z):
         gradients(g)
+    for k in range(3):
+        stored[k].start()
     ret[slot_rows(0), :] = ret_out[slot_rows(0), :]
 
-    def take_back(r, carry):
-        give_back(r).wait_recv()
-        return carry
-
-    lax.fori_loop(1, n_sp, take_back, 0)
+    others = ret.at[cap:, :]
+    remote(others, others, back_s, back_r, partner).wait_recv()
     mixed = (out_cot[...].astype(f32) + dot_nn(sel_t[...], ret[...])).astype(bf16)
     full_cot[tp] = mixed
 
@@ -549,10 +578,15 @@
         return remote(
             pj_out.at[j],
             pj_in.at[sp, lax.rem(j, wide)],
-            pj_s.at[j],
-            pj_r.at[sp, lax.rem(j, wide)],
+            pj_s,
+            pj_r,
             (j // wide, tp),
         )
+
+    def proj_send(j):
+        @pl.when(j // wide != sp)
+        def _():
+            proj_copy(j).start()
 
     def project(b, p):
         at = pl.ds(pl.multiple_of(p * tok_half, tok_half), tok_half)
@@ -571,11 +605,13 @@
                 def _():
                     pj_in[sp, lax.rem(j, wide)] = pj_out[j]
 
-                @pl.when(j // wide != sp)
+                away = lax.rem(b - z + n_z, n_z)
+
+                @pl.when((away < half - 1) | (away > half + 1))
                 def _():
-                    proj_copy(j).start()
-
-    drain_toks = ring(
+                    proj_send(j)
+
+    ring(
         2,
         lambda block, p: full_cot.at[block, pl.ds(pl.multiple_of(p * tok_half, tok_half), tok_half), :],
         tk_s,
@@ -590,82 +626,98 @@
     cot = mixer_cot[...]
     fut = fine(dot_tn, q_dec[...], cot)
     fut_out[...] = fut.astype(bf16)
-    to_peers(future_copy)
+    lax.fori_loop(1, n_sp, to_earlier, 0)
+    for d in (half - 1, half, half + 1):
+        for i in range(2):
+            proj_send(2 * zpos(d) + i)
     cot_values = jnp.where(causal, fine(dot_nt, cot, value[...]), 0.0)
     cum = cumul[...]
     q_grad = jnp.exp(cum) * (fine(dot_nt, cot, entry[...]) + fine(dot_nn, cot_values, k_back[...]))
-    query_g[...] = q_grad * DK ** (-0.5)
+    query_g[...] = (q_grad * DK ** (-0.5)).T
     key_part = jnp.exp(-cum) * fine(dot_tn, cot_values, q_dec[...])
     value_g[...] = fine(dot_tn, scores[...], cot)
 
-    def fut_arrived(r, carry):
-        future_copy(r).wait_recv()
+    def fut_arrived(s, carry):
+        @pl.when(s > sp)
+        def _():
+            remote(fut_out, fut_in.at[s], bw_s.at[0], bw_r.at[s], partner).wait_recv()
+
         return carry
 
-    lax.fori_loop(1, n_sp, fut_arrived, 0)
+    lax.fori_loop(0, n_sp, fut_arrived, 0)
 
     def pass_back(i, state):
         s = n_sp - 1 - i
-        return jnp.where(
-            s > sp, span_in[s, DK : 2 * DK, :] * state + fut_in[s].astype(f32), state
-        )
+        later_on = span_in[s, DK : 2 * DK, :] * state + fut_in[s].astype(f32)
+        return jnp.where(s > sp, later_on, state)
 
     future = lax.fori_loop(0, n_sp, pass_back, jnp.zeros((DK, DV), f32))
     k_grad = key_part + jnp.exp(cum[toks - 1 : toks, :] - cum) * fine(dot_nt, value[...], future)
-    key_g[...] = k_grad
+    k_grad_t = k_grad.T
+    key_g[...] = k_grad_t
     value_g[...] += fine(dot_nn, k_end[...], future)
     span_end = span_out[DK : 2 * DK, :] * entry[...] + span_out[0:DK, :]
-    beyond = fine(dot_nt, jnp.ones((8, DV), bf16), future * span_end, 3)[0:1, :]
-    terms = query[...].astype(f32) * DK ** (-0.5) * q_grad - key_in[...].astype(f32) * k_grad
-    since = jnp.where(t_col >= t_row, 1.0, 0.0).astype(bf16)
-    tail = fine(dot_nn, since, terms, 3) + beyond
+    beyond = jnp.sum(future * span_end, axis=1, keepdims=True)
+    terms = query[...].astype(f32) * query_g[...] - key_in[...].astype(f32) * k_grad_t
+    since = jnp.where(t_row >= t_col, 1.0, 0.0).astype(bf16)
+    tail = fine(dot_nn, terms, since, 3) + beyond
     logit_g[...] = tail * jax.nn.sigmoid(-logit[...].astype(f32)) / decay_temp
 
-    def proj_arrived(s, carry):
-        for i in range(wide):
-            @pl.when(s != sp)
-            def _():
-                remote(
-                    pj_out.at[0], pj_in.at[s, i], pj_s.at[0], pj_r.at[s, i], (sp, tp)
-                ).wait_recv()
-
-        return carry
-
-    lax.fori_loop(0, n_sp, proj_arrived, 0)
+    came = pj_in.at[1:]
+    remote(came, came, pj_s, pj_r, partner).wait_recv()
     for i in range(wide):
         sums = jnp.zeros((128, cols), f32)
         for s in range(n_sp):
             sums = sums + pj_in[s, i].astype(f32)
         proj_g[i * cols : (i + 1) * cols, :] = sums.T
 
-    def sent(r, carry):
-        dispatch(r).wait_send()
-        give_back(r).wait_send()
-        span_copy(r).wait_send()
-        future_copy(r).wait_send()
+    for k in range(3, 8):
+        stored[k].start()
+
+    for copy in give_w:
+        copy.wait_send()
+
+    def fut_sent(r, carry):
+        @pl.when(there(r) < sp)
+        def _():
+            future_copy(r).wait_send()
+
         return carry
 
-    lax.fori_loop(1, n_sp, sent, 0)
-    for copy in (*give_w, give_gu):
-        copy.wait_send()
-
-    def sums_sent(k, carry):
-        for d in range(2):
-            hop_sum(d, k).wait_send()
-        return carry
-
-    lax.fori_loop(0, rs_total, sums_sent, 0)
-
-    def proj_sent(j, carry):
-        @pl.when(j // wide != sp)
-        def _():
-            proj_copy(j).wait_send()
-
-        return carry
-
-    lax.fori_loop(0, 2 * n_z, proj_sent, 0)
-    drain_rows()
-    drain_toks()
+    lax.fori_loop(1, n_sp, fut_sent, 0)
+    for sent, sem in (
+        (send.at[:, cap:, :], a2a_s),
+        (ret.at[cap:, :], back_s),
+        (span_in.at[1:], fw_s),
+        (pj_in.at[1:], pj_s),
+        (rows.at[: n_z - 1], ag_s),
+        (rows.at[:n_z], agd_s),
+        (full_cot.at[: n_z - 1], tk_s),
+        (full_cot.at[:n_z], tkd_s),
+        (stage, rs_s),
+        (gu, gu_s),
+    ):
+        remote(sent, sent, sem, back_r, partner).wait_send()
+    for copy in stored:
+        copy.wait()
+
+
+def store_kernel(*refs):
+    taken = [
+        pltpu.make_async_copy(source, target, refs[24].at[k])
+        for k, (source, target) in enumerate(zip(refs[:8], refs[16:24]))
+    ]
+    stored = [
+        pltpu.make_async_copy(source, target, refs[25].at[k])
+        for k, (source, target) in enumerate(zip(refs[16:24], refs[8:16]))
+    ]
+    for copy in taken:
+        copy.start()
+    for first, second in zip(taken, stored):
+        first.wait()
+        second.start()
+    for copy in stored:
+        copy.wait()
 
 
 def local(
@@ -697,21 +749,26 @@
     wide = n_tp // n_sp
     dma = pltpu.SemaphoreType.DMA
     vmem = pl.BlockSpec(memory_space=pltpu.VMEM)
-    gate_g, up_g, down_g, *rest = pl.pallas_call(
+    hbm = pl.BlockSpec(memory_space=pltpu.HBM)
+    small = (DK, toks)
+    shapes = ((128, width),) * 3 + ((wide * cols, DV), small, small, (toks, DV), small)
+    grads = pl.pallas_call(
         functools.partial(moe_kernel, (n_sp, n_x, n_z, pieces)),
-        out_shape=(
-            jax.ShapeDtypeStruct((128, width), f32),
-            jax.ShapeDtypeStruct((128, width), f32),
-            jax.ShapeDtypeStruct((128, width), f32),
-            jax.ShapeDtypeStruct((wide * cols, DV), f32),
-            jax.ShapeDtypeStruct((toks, DK), f32),
-            jax.ShapeDtypeStruct((toks, DK), f32),
-            jax.ShapeDtypeStruct((toks, DV), f32),
-            jax.ShapeDtypeStruct((toks, DK), f32),
-        ),
-        in_specs=[vmem] * 13,
-        out_specs=[vmem] * 8,
+        out_shape=tuple(jax.ShapeDtypeStruct(shape, f32) for shape in shapes),
+        in_specs=[vmem] * 3 + [hbm] * 10,
+        out_specs=[hbm] * 8,
         scratch_shapes=[
+            pltpu.VMEM((toks, cols), bf16),
+            pltpu.VMEM((toks, cols), bf16),
+            pltpu.VMEM((128, width), bf16),
+            pltpu.VMEM((128, width), bf16),
+            pltpu.VMEM((128, width), bf16),
+            pltpu.VMEM((width, DV), bf16),
+            pltpu.VMEM((DK, toks), bf16),
+            pltpu.VMEM((DK, toks), bf16),
+            pltpu.VMEM((toks, DV), bf16),
+            pltpu.VMEM((DK, toks), bf16),
+            *(pltpu.VMEM(shape, f32) for shape in shapes),
             pltpu.VMEM((n_tp, toks, cols), bf16),
             pltpu.VMEM((toks, DV), f32),
             pltpu.VMEM((toks, DK), f32),
@@ -741,48 +798,69 @@
             pltpu.VMEM((2, total, chunk, cols), bf16),
             pltpu.VMEM((n_rows, cols), bf16),
             pltpu.VMEM((n_rows, cols), bf16),
+            dma(()),
+            dma((pieces,)),
+            dma(()),
+            dma(()),
+            dma(()),
+            dma((2, total)),
+            dma(()),
+            dma((pieces + 2 * total,)),
+            dma(()),
+            dma((2, total)),
+            dma(()),
+            dma((2, tk_total)),
+            dma(()),
+            dma((2 + 2 * tk_total,)),
+            dma((2,)),
+            dma((2,)),
+            dma(()),
+            dma((pieces,)),
+            dma(()),
+            dma(()),
             dma((n_sp,)),
             dma((n_sp,)),
-            dma((n_sp,)),
-            dma((n_sp,)),
-            dma((2, total)),
-            dma((2, total)),
-            dma((pieces + 2 * total,)),
-            dma((pieces + 2 * total,)),
-            dma((2, total)),
-            dma((2, total)),
-            dma((2, tk_total)),
-            dma((2, tk_total)),
-            dma((2 + 2 * tk_total,)),
-            dma((2 + 2 * tk_total,)),
-            dma((3,)),
-            dma((3,)),
-            dma((n_sp,)),
-            dma((n_sp,)),
-            dma((n_sp,)),
-            dma((n_sp,)),
-            dma((n_tp,)),
-            dma((n_sp, wide)),
+            dma(()),
+            dma(()),
+            dma((10,)),
+            dma((8,)),
         ],
         compiler_params=pltpu.CompilerParams(
             collective_id=0, has_side_effects=True, vmem_limit_bytes=60 * 1024 * 1024
         ),
     )(
+        route_ids.T,
+        route_probs.T,
+        group_prob,
         layer_in,
         out_cot,
-        route_ids.T,
-        route_probs.T,
-        group_prob.reshape(1, toks),
         gate_weight[0],
         up_weight[0],
         down_weight[0],
         out_weight,
-        query,
-        key_in,
+        query.T,
+        key_in.T,
         value,
-        decay_logit,
+        decay_logit.T,
     )
-    return (gate_g[None], up_g[None], down_g[None], *rest)
+    gate_g, up_g, down_g, proj_g, query_g, key_g, value_g, logit_g = pl.pallas_call(
+        store_kernel,
+        out_shape=tuple(jax.ShapeDtypeStruct(g.shape, g.dtype) for g in grads),
+        in_specs=[hbm] * 8,
+        out_specs=[hbm] * 8,
+        scratch_shapes=[*(pltpu.VMEM(g.shape, g.dtype) for g in grads), dma((8,)), dma((8,))],
+        compiler_params=pltpu.CompilerParams(vmem_limit_bytes=60 * 1024 * 1024),
+    )(*grads)
+    return (
+        gate_g[None],
+        up_g[None],
+        down_g[None],
+        proj_g,
+        query_g.T,
+        key_g.T,
+        value_g,
+        logit_g.T,
+    )
 
 
 def solution(mesh):

time: 150 us -> 134 us (0.89); the launches traced: 148 us -> 134 us
  local copies, waits for them, and re-layouts: 14 us -> 0 us
    unnamed x29 -> x0, local copies, waits for them, and re-layouts: 13.4 us -> none
    pallas_call x1, Pallas kernels: 133 us -> 130 us  [local(): pl.pallas_call(functools.partial(moe_kernel, (n_sp, n_x, n_z, pieces)), o...]
    pallas_call x0 -> x1, Pallas kernels: none -> 3.18 us  [local(): pl.pallas_call(store_kernel, out_shape=tuple((jax.ShapeDtypeStruct(g.shap...]
where the time goes in v3:
time: 134 us
  Pallas kernels  133 us (99%)
    pallas_call x1, Pallas kernels, local(): pl.pallas_call(functools.partial(moe_kernel, (n_sp, n_x, n_z, pieces)), o...  130 us
    pallas_call x1, Pallas kernels, local(): pl.pallas_call(store_kernel, out_shape=tuple((jax.ShapeDtypeStruct(g.shap...  3.18 us

profile of v3, /device:TPU:96, one launch (start us, length us, event | category | flops | bytes accessed | tf_op | source)
XLA Modules:
  0.0 133.8 jit_solution(13835517800571194193)
XLA Ops:
  0.6 129.9 %shard_map.188 = (f32[128,2048]{1,0:T(8,128)}, f32[128,2048]{1,0:T(8,128)}, f32[128,2048]{1,0:T(8,128)}, f32[128,128]{1,0:T(8,128)}, f32[64,320]{1,0:T(8,128)}, ...) custom-call(s32[2,320]{1,0:T(2,128)} %bitcast.20, f32[2,320]{1,0:T(2,128)} %bitcast.21, f32[320]{0:T(512)} %group.1, ...), custom_call_target="tpu_custom_call" | custom-call | tf_op jit(solution)/shard_map/pallas_call | solution.py:755
  130.6 3.2 %shard_map.189 = (f32[128,2048]{1,0:T(8,128)}, f32[128,2048]{1,0:T(8,128)}, f32[128,2048]{1,0:T(8,128)}, f32[128,128]{1,0:T(8,128)}, f32[64,320]{1,0:T(8,128)}, ...) custom-call(f32[128,2048]{1,0:T(8,128)} %get-tuple-element.24.refs_0_, ...), custom_call_target="tpu_custom_call" | custom-call | tf_op jit(solution)/shard_map/pallas_call | solution.py:846

commit v4 on v3

--- a/solution.py
+++ b/solution.py
@@ -168,6 +168,8 @@
     z_dn = lax.rem(z + n_z - 1, n_z)
     partner = (sp, 2 * z + 1 - core)
     above, below = (sp, 2 * z_up + core), (sp, 2 * z_dn + core)
+    two_up = (sp, 2 * lax.rem(z + 2, n_z) + core)
+    two_dn = (sp, 2 * lax.rem(z + n_z - 2, n_z) + core)
     my_y, my_x = sp // n_x, lax.rem(sp, n_x)
 
     def there(r):
@@ -189,7 +191,8 @@
     barrier = pltpu.get_barrier_semaphore()
     for r in range(1, n_sp):
         pl.semaphore_signal(barrier, inc=1, device_id=(there(r), tp), device_id_type=MESH)
-    for dev in (partner, above, below):
+    greeted = (partner, above, below) + ((two_up, two_dn) if half == 4 else ())
+    for dev in greeted:
         pl.semaphore_signal(barrier, inc=1, device_id=dev, device_id_type=MESH)
 
     t_row = lax.broadcasted_iota(jnp.int32, (toks, toks), 0)
@@ -243,7 +246,7 @@
         return carry
 
     lax.fori_loop(0, pieces, select, 0)
-    pl.semaphore_wait(barrier, n_sp + 2)
+    pl.semaphore_wait(barrier, n_sp - 1 + len(greeted))
 
     give_w = [
         remote(w, part_w.at[k], misc_s.at[k], misc_r.at[k], partner)
@@ -275,13 +278,13 @@
 
     last = (half - 1) * pieces
 
-    def ring(n_pieces, where, sems_s, sems_r, sems_ds, sems_dr, own_ready, compute, beside):
+    def ring(n_pieces, where, sems_s, sems_r, sems_ds, sems_dr, own_ready, compute, beside, stop, leap):
         h_p = n_pieces // 2
         total = (half - 1) * n_pieces + h_p
 
-        def along(block, p, d, k):
+        def along(block, p, d, k, far=False):
             ref = where(block, p)
-            return remote(ref, ref, sems_s, sems_r.at[d, k], above if d == 0 else below)
+            return remote(ref, ref, sems_s, sems_r.at[d, k], (two_up, two_dn)[d] if far else (above, below)[d])
 
         def across(block, p, k):
             ref = where(block, p)
@@ -289,6 +292,9 @@
 
         def own(p, carry):
             own_ready(p)
+            if leap:
+                along(tp, p, 0, n_pieces + p, True).start()
+                along(tp, p, 1, n_pieces + p, True).start()
             along(tp, p, 0, p).start()
             along(tp, p, 1, p).start()
             across(tp, p, p).start()
@@ -311,31 +317,50 @@
             hop = t // n_pieces
             return hop, p_up, p_dn
 
-        def step(t, carry):
+        def move(t):
             hop, p_up, p_dn = at(t)
             b_up, b_dn = zpos(-1 - hop), zpos(1 + hop)
             along(2 * b_up + core, p_up, 0, t).wait_recv()
-
-            @pl.when((hop < half - 2) | ((hop == half - 2) & (p_up < h_p)))
+            pass_up = (hop < half - 2) | ((hop == half - 2) & (p_up < h_p))
+
+            @pl.when((hop == 1) if leap else pass_up)
             def _():
                 along(2 * b_up + core, p_up, 0, t + n_pieces).start()
 
+            if leap:
+                @pl.when((hop == 1) & (p_up < h_p))
+                def _():
+                    along(2 * b_up + core, p_up, 0, t + 2 * n_pieces, True).start()
+
             across(2 * b_up + core, p_up, n_pieces + 2 * t).start()
             along(2 * b_dn + core, p_dn, 1, t).wait_recv()
 
-            @pl.when(hop < half - 2)
+            @pl.when((hop == 1) if leap else (hop < half - 2))
             def _():
                 along(2 * b_dn + core, p_dn, 1, t + n_pieces).start()
 
-            @pl.when((hop == half - 2) & (p_dn >= h_p))
+            if leap:
+                @pl.when((hop == 1) & (p_dn >= h_p))
+                def _():
+                    along(2 * b_dn + core, p_dn, 1, t + 2 * n_pieces - h_p, True).start()
+            else:
+                @pl.when((hop == half - 2) & (p_dn >= h_p))
+                def _():
+                    along(2 * b_dn + core, p_dn, 1, t + n_pieces - h_p).start()
+
+            across(2 * b_dn + core, p_dn, n_pieces + 2 * t + 1).start()
+
+        def turn(u):
+            if not leap:
+                return u
+            return jnp.where(u < n_pieces, u + n_pieces, jnp.where(u < 2 * n_pieces, u - n_pieces, u))
+
+        def step(u, carry):
+            move(turn(u))
+
+            @pl.when(u > 0)
             def _():
-                along(2 * b_dn + core, p_dn, 1, t + n_pieces - h_p).start()
-
-            across(2 * b_dn + core, p_dn, n_pieces + 2 * t + 1).start()
-
-            @pl.when(t > 0)
-            def _():
-                use(t - 1)
+                use(turn(u - 1))
 
             return carry
 
@@ -347,8 +372,9 @@
             across(2 * b_dn + 1 - core, p_dn, n_pieces + 2 * t + 1).wait_recv()
             compute(b_dn, p_dn)
 
-        lax.fori_loop(0, total, step, 0)
-        use(total - 1)
+        lax.fori_loop(0, total - stop, step, 0)
+        use(total - stop - 1)
+        return move, use
 
 
     def piece_rows(p):
@@ -431,7 +457,8 @@
         pre[at, 0:256] += dot_nt(x, w_gu)
         pre[at, 256:384] += dot_nt(c, down[:, feats(b)])
 
-    ring(
+    early = 1 if pieces == 4 else 0
+    move, use = ring(
         pieces,
         lambda block, p: rows.at[block, :, piece_rows(p), :],
         ag_s,
@@ -441,6 +468,8 @@
         rows_ready,
         expert_in,
         attend,
+        early,
+        False,
     )
 
     h_p = pieces // 2
@@ -461,10 +490,6 @@
         pre[at, 0:128] = active * up_pre
         return carry
 
-    lax.fori_loop(0, pieces, middle, 0)
-    for copy in give_w:
-        copy.wait_recv()
-
     rs_total = h_p + (half - 1) * pieces
 
     def partial(b, p):
@@ -490,7 +515,20 @@
             hop_sum(d, t).start()
         return carry
 
-    lax.fori_loop(0, h_p, first, 0)
+    if early:
+        lax.fori_loop(0, 2, middle, 0)
+        for copy in give_w:
+            copy.wait_recv()
+        move(rs_total - 1)
+        first(0, 0)
+        use(rs_total - 1)
+        lax.fori_loop(2, pieces, middle, 0)
+        lax.fori_loop(1, h_p, first, 0)
+    else:
+        lax.fori_loop(0, pieces, middle, 0)
+        for copy in give_w:
+            copy.wait_recv()
+        lax.fori_loop(0, h_p, first, 0)
     gu_t[...] = gu[...].T
     hid_t[...] = pre[:, 0:128].astype(bf16).T
     enter()
@@ -569,7 +607,8 @@
     mixed = (out_cot[...].astype(f32) + dot_nn(sel_t[...], ret[...])).astype(bf16)
     full_cot[tp] = mixed
 
-    tok_half = toks // 2
+    tok_pieces = 4 if pieces == 4 else 2
+    tok_rows = toks // tok_pieces
     mixer_cot[...] = jnp.zeros_like(mixer_cot)
 
     wide = 2 * n_z // n_sp
@@ -589,13 +628,10 @@
             proj_copy(j).start()
 
     def project(b, p):
-        at = pl.ds(pl.multiple_of(p * tok_half, tok_half), tok_half)
-        c = jnp.concatenate([full_cot[2 * b, at, :], full_cot[2 * b + 1, at, :]], axis=1)
-        mixer_cot[at, :] += dot_nn(c, out_w[feats(b), :])
-
-        @pl.when(p == 1)
+        @pl.when(p == tok_pieces - 1)
         def _():
             whole = jnp.concatenate([full_cot[2 * b], full_cot[2 * b + 1]], axis=1)
+            mixer_cot[...] += dot_nn(whole, out_w[feats(b), :])
             found = dot_nn(mix_t[...], whole).astype(bf16)
             for i in range(2):
                 j = 2 * b + i
@@ -607,13 +643,13 @@
 
                 away = lax.rem(b - z + n_z, n_z)
 
-                @pl.when((away < half - 1) | (away > half + 1))
+                @pl.when(away != half)
                 def _():
                     proj_send(j)
 
     ring(
-        2,
-        lambda block, p: full_cot.at[block, pl.ds(pl.multiple_of(p * tok_half, tok_half), tok_half), :],
+        tok_pieces,
+        lambda block, p: full_cot.at[block, pl.ds(pl.multiple_of(p * tok_rows, tok_rows), tok_rows), :],
         tk_s,
         tk_r,
         tkd_s,
@@ -621,15 +657,16 @@
         lambda p: None,
         project,
         lambda: None,
+        0,
+        half == 4,
     )
 
     cot = mixer_cot[...]
     fut = fine(dot_tn, q_dec[...], cot)
     fut_out[...] = fut.astype(bf16)
     lax.fori_loop(1, n_sp, to_earlier, 0)
-    for d in (half - 1, half, half + 1):
-        for i in range(2):
-            proj_send(2 * zpos(d) + i)
+    for i in range(2):
+        proj_send(2 * zpos(half) + i)
     cot_values = jnp.where(causal, fine(dot_nt, cot, value[...]), 0.0)
     cum = cumul[...]
     q_grad = jnp.exp(cum) * (fine(dot_nt, cot, entry[...]) + fine(dot_nn, cot_values, k_back[...]))
@@ -744,7 +781,8 @@
     width = gate_weight.shape[2]
     n_rows = 4 * toks
     total = (half - 1) * pieces + pieces // 2
-    tk_total = (half - 1) * 2 + 1
+    tk_pieces = 4 if pieces == 4 else 2
+    tk_total = (half - 1) * tk_pieces + tk_pieces // 2
     chunk = n_rows // pieces
     wide = n_tp // n_sp
     dma = pltpu.SemaphoreType.DMA
@@ -811,7 +849,7 @@
             dma(()),
             dma((2, tk_total)),
             dma(()),
-            dma((2 + 2 * tk_total,)),
+            dma((tk_pieces + 2 * tk_total,)),
             dma((2,)),
             dma((2,)),
             dma(()),

time: 134 us -> 130 us (0.970)
  Pallas kernels: 133 us -> 128 us
    pallas_call x1, Pallas kernels: 130 us -> 125 us  [local(): pl.pallas_call(functools.partial(moe_kernel, (n_sp, n_x, n_z, pieces)), o...]
where the time goes in v4:
time: 130 us; the launch traced here: 129 us
  Pallas kernels  128 us (98%)
    pallas_call x1, Pallas kernels, local(): pl.pallas_call(functools.partial(moe_kernel, (n_sp, n_x, n_z, pieces)), o...  125 us
    pallas_call x1, Pallas kernels, local(): pl.pallas_call(store_kernel, out_shape=tuple((jax.ShapeDtypeStruct(g.shap...  3.18 us

profile of v4, /device:TPU:96, one launch (start us, length us, event | category | flops | bytes accessed | tf_op | source)
XLA Modules:
  0.0 128.6 jit_solution(18359594456572270533)
XLA Ops:
  0.6 124.7 %shard_map.188 = (f32[128,2048]{1,0:T(8,128)}, f32[128,2048]{1,0:T(8,128)}, f32[128,2048]{1,0:T(8,128)}, f32[128,128]{1,0:T(8,128)}, f32[64,320]{1,0:T(8,128)}, ...) custom-call(s32[2,320]{1,0:T(2,128)} %bitcast.20, f32[2,320]{1,0:T(2,128)} %bitcast.21, f32[320]{0:T(512)} %group.1, ...), custom_call_target="tpu_custom_call" | custom-call | tf_op jit(solution)/shard_map/pallas_call | solution.py:793
  125.4 3.2 %shard_map.189 = (f32[128,2048]{1,0:T(8,128)}, f32[128,2048]{1,0:T(8,128)}, f32[128,2048]{1,0:T(8,128)}, f32[128,128]{1,0:T(8,128)}, f32[64,320]{1,0:T(8,128)}, ...) custom-call(f32[128,2048]{1,0:T(8,128)} %get-tuple-element.24.refs_0_, ...), custom_call_target="tpu_custom_call" | custom-call | tf_op jit(solution)/shard_map/pallas_call | solution.py:884

commit v5 on v4

--- a/solution.py
+++ b/solution.py
@@ -221,10 +221,6 @@
 
     slot0 = offset_of(id0) * cap + pos0.astype(jnp.int32)
     slot1 = offset_of(id1) * cap + pos1.astype(jnp.int32)
-    slots = lax.broadcasted_iota(jnp.int32, (toks, n_rows), 1)
-    sel_t[...] = (
-        jnp.where(slots == slot0, 1.0, 0.0) + jnp.where(slots == slot1, 1.0, 0.0)
-    ).astype(bf16)
     p0, p1 = probs[0:1, :], probs[1:2, :]
     group_row = group[...].reshape(1, toks)
     w0 = group_row * p0 / (p0 + p1)
@@ -245,8 +241,38 @@
         send[1, pl.ds(base, chunk), :] = (picked[:, cols:] * weight).astype(bf16)
         return carry
 
-    lax.fori_loop(0, pieces, select, 0)
+    select(0, 0)
     pl.semaphore_wait(barrier, n_sp - 1 + len(greeted))
+
+    def slot_rows(r):
+        return pl.ds(pl.multiple_of(r * cap, cap), cap)
+
+    def dispatch(r):
+        return remote(
+            send.at[:, slot_rows(r), :],
+            rows.at[tp, :, slot_rows(r), :],
+            a2a_s,
+            a2a_r.at[r // per],
+            (there(r), tp),
+        )
+
+    def start_dispatch(p):
+        for i in range(per):
+            r = p * per + i
+
+            @pl.when(r > 0)
+            def _():
+                dispatch(r).start()
+
+    start_dispatch(0)
+
+    def select_next(p, carry):
+        select(p, 0)
+        start_dispatch(p)
+        return carry
+
+    lax.fori_loop(1, pieces, select_next, 0)
+    rows[tp, :, slot_rows(0), :] = send[:, slot_rows(0), :]
 
     give_w = [
         remote(w, part_w.at[k], misc_s.at[k], misc_r.at[k], partner)
@@ -256,25 +282,6 @@
     loaded[3].wait()
     for copy in give_w:
         copy.start()
-
-    def slot_rows(r):
-        return pl.ds(pl.multiple_of(r * cap, cap), cap)
-
-    def dispatch(r):
-        return remote(
-            send.at[:, slot_rows(r), :],
-            rows.at[tp, :, slot_rows(r), :],
-            a2a_s,
-            a2a_r.at[r // per],
-            (there(r), tp),
-        )
-
-    def start_dispatch(r, carry):
-        dispatch(r).start()
-        return carry
-
-    lax.fori_loop(1, n_sp, start_dispatch, 0)
-    rows[tp, :, slot_rows(0), :] = send[:, slot_rows(0), :]
 
     last = (half - 1) * pieces
 
@@ -417,6 +424,10 @@
         return carry
 
     def attend():
+        slots = lax.broadcasted_iota(jnp.int32, (toks, n_rows), 1)
+        sel_t[...] = (
+            jnp.where(slots == slot0, 1.0, 0.0) + jnp.where(slots == slot1, 1.0, 0.0)
+        ).astype(bf16)
         for k in (6, 7, 8, 9, 4, 5):
             loaded[k].wait()
         log_decay = jax.nn.log_sigmoid(logit[...].astype(f32).T) / decay_temp
@@ -604,11 +615,18 @@
 
     others = ret.at[cap:, :]
     remote(others, others, back_s, back_r, partner).wait_recv()
-    mixed = (out_cot[...].astype(f32) + dot_nn(sel_t[...], ret[...])).astype(bf16)
-    full_cot[tp] = mixed
 
     tok_pieces = 4 if pieces == 4 else 2
     tok_rows = toks // tok_pieces
+
+    def tok_at(p):
+        return pl.ds(pl.multiple_of(p * tok_rows, tok_rows), tok_rows)
+
+    def mix(p):
+        at = tok_at(p)
+        routed = dot_nn(sel_t[at, :], ret[...])
+        full_cot[tp, at, :] = (out_cot[at, :].astype(f32) + routed).astype(bf16)
+
     mixer_cot[...] = jnp.zeros_like(mixer_cot)
 
     wide = 2 * n_z // n_sp
@@ -649,12 +667,12 @@
 
     ring(
         tok_pieces,
-        lambda block, p: full_cot.at[block, pl.ds(pl.multiple_of(p * tok_rows, tok_rows), tok_rows), :],
+        lambda block, p: full_cot.at[block, tok_at(p), :],
         tk_s,
         tk_r,
         tkd_s,
         tkd_r,
-        lambda p: None,
+        mix,
         project,
         lambda: None,
         0,

time: 130 us -> 130 us (level)
  no operation moved by 1% of the time
where the time goes in v5:
time: 130 us; the launch traced here: 128 us
  Pallas kernels  128 us (98%)
    pallas_call x1, Pallas kernels, local(): pl.pallas_call(functools.partial(moe_kernel, (n_sp, n_x, n_z, pieces)), o...  124 us
    pallas_call x1, Pallas kernels, local(): pl.pallas_call(store_kernel, out_shape=tuple((jax.ShapeDtypeStruct(g.shap...  3.18 us

profile of v5, /device:TPU:96, one launch (start us, length us, event | category | flops | bytes accessed | tf_op | source)
XLA Modules:
  0.0 128.2 jit_solution(7086576361441018349)
XLA Ops:
  0.6 124.4 %shard_map.188 = (f32[128,2048]{1,0:T(8,128)}, f32[128,2048]{1,0:T(8,128)}, f32[128,2048]{1,0:T(8,128)}, f32[128,128]{1,0:T(8,128)}, f32[64,320]{1,0:T(8,128)}, ...) custom-call(s32[2,320]{1,0:T(2,128)} %bitcast.20, f32[2,320]{1,0:T(2,128)} %bitcast.21, f32[320]{0:T(512)} %group.1, ...), custom_call_target="tpu_custom_call" | custom-call | tf_op jit(solution)/shard_map/pallas_call | solution.py:811
  125.0 3.2 %shard_map.189 = (f32[128,2048]{1,0:T(8,128)}, f32[128,2048]{1,0:T(8,128)}, f32[128,2048]{1,0:T(8,128)}, f32[128,128]{1,0:T(8,128)}, f32[64,320]{1,0:T(8,128)}, ...) custom-call(f32[128,2048]{1,0:T(8,128)} %get-tuple-element.24.refs_0_, ...), custom_call_target="tpu_custom_call" | custom-call | tf_op jit(solution)/shard_map/pallas_call | solution.py:902

commit v6 on v5

--- a/solution.py
+++ b/solution.py
@@ -101,6 +101,8 @@
     pj_out,
     pj_in,
     send,
+    near,
+    send_near,
     sel_t,
     rows,
     pre,
@@ -131,6 +133,10 @@
     misc_r,
     gu_s,
     gu_r,
+    tok_s,
+    tok_r,
+    nb_s,
+    nb_r,
     fw_s,
     fw_r,
     bw_s,
@@ -172,12 +178,15 @@
     two_dn = (sp, 2 * lax.rem(z + n_z - 2, n_z) + core)
     my_y, my_x = sp // n_x, lax.rem(sp, n_x)
 
+    def row_of(k):
+        return jnp.where(k == 1, 2, jnp.where(k == 2, 1, k)) if n_y == 4 else k
+
     def there(r):
-        ry, rx = r // n_x, lax.rem(r, n_x)
+        ry, rx = row_of(r // n_x), lax.rem(r, n_x)
         return lax.rem(my_y + ry, n_y) * n_x + lax.rem(my_x + rx, n_x)
 
     def back_to(r):
-        ry, rx = r // n_x, lax.rem(r, n_x)
+        ry, rx = row_of(r // n_x), lax.rem(r, n_x)
         return lax.rem(my_y + n_y - ry, n_y) * n_x + lax.rem(my_x + n_x - rx, n_x)
 
     def zpos(d):
@@ -194,6 +203,9 @@
     greeted = (partner, above, below) + ((two_up, two_dn) if half == 4 else ())
     for dev in greeted:
         pl.semaphore_signal(barrier, inc=1, device_id=dev, device_id_type=MESH)
+
+    def piece_rows(p):
+        return pl.ds(pl.multiple_of(p * chunk, chunk), chunk)
 
     t_row = lax.broadcasted_iota(jnp.int32, (toks, toks), 0)
     t_col = lax.broadcasted_iota(jnp.int32, (toks, toks), 1)
@@ -217,7 +229,7 @@
 
     def offset_of(expert):
         ey, ex = expert // n_x, lax.rem(expert, n_x)
-        return lax.rem(ey + n_y - my_y, n_y) * n_x + lax.rem(ex + n_x - my_x, n_x)
+        return row_of(lax.rem(ey + n_y - my_y, n_y)) * n_x + lax.rem(ex + n_x - my_x, n_x)
 
     slot0 = offset_of(id0) * cap + pos0.astype(jnp.int32)
     slot1 = offset_of(id1) * cap + pos1.astype(jnp.int32)
@@ -230,19 +242,32 @@
     loaded[1].wait()
     both = jnp.concatenate([layer_in[...], out_cot[...]], axis=1)
 
-    def select(p, carry):
-        base = pl.multiple_of(p * chunk, chunk)
+    def picking(p):
         here = (lax.broadcasted_iota(jnp.int32, (chunk, toks), 0) + p * chunk).astype(f32)
         m0, m1 = here == slot0_row, here == slot1_row
         pick = (jnp.where(m0, 1.0, 0.0) + jnp.where(m1, 1.0, 0.0)).astype(bf16)
         weight = jnp.sum(jnp.where(m0, w0, 0.0) + jnp.where(m1, w1, 0.0), axis=1, keepdims=True)
+        return pick, weight
+
+    def select(p, carry):
+        pick, weight = picking(p)
         picked = dot_nn(pick, both)
-        send[0, pl.ds(base, chunk), :] = picked[:, :cols].astype(bf16)
-        send[1, pl.ds(base, chunk), :] = (picked[:, cols:] * weight).astype(bf16)
+        send[0, piece_rows(p), :] = picked[:, :cols].astype(bf16)
+        send[1, piece_rows(p), :] = (picked[:, cols:] * weight).astype(bf16)
         return carry
 
     select(0, 0)
     pl.semaphore_wait(barrier, n_sp - 1 + len(greeted))
+
+    def give_tok(d):
+        return [
+            remote(source, near.at[1 - d, k], tok_s, tok_r.at[1 - d], below if d == 0 else above)
+            for k, source in enumerate((layer_in, out_cot))
+        ]
+
+    for d in range(2):
+        for copy in give_tok(d):
+            copy.start()
 
     def slot_rows(r):
         return pl.ds(pl.multiple_of(r * cap, cap), cap)
@@ -274,6 +299,44 @@
     lax.fori_loop(1, pieces, select_next, 0)
     rows[tp, :, slot_rows(0), :] = send[:, slot_rows(0), :]
 
+    through = pieces // 2
+    nb_tp = (2 * z_dn + core, 2 * z_up + core)
+
+    def dispatch_near(r, d):
+        return remote(
+            send_near.at[d, :, slot_rows(r), :],
+            rows.at[nb_tp[d], :, slot_rows(r), :],
+            nb_s,
+            nb_r.at[d, r // per],
+            (there(r), tp),
+        )
+
+    def near_rows():
+        for d in range(2):
+            remote(near.at[d], near.at[d], tok_s, tok_r.at[d], partner).wait_recv()
+        tokens = jnp.concatenate([near[0, 0], near[0, 1], near[1, 0], near[1, 1]], axis=1)
+
+        def one(p, carry):
+            pick, weight = picking(p)
+            picked = dot_nn(pick, tokens)
+            for d in range(2):
+                x = picked[:, 2 * d * cols : (2 * d + 1) * cols]
+                c = picked[:, (2 * d + 1) * cols : (2 * d + 2) * cols]
+                send_near[d, 0, piece_rows(p), :] = x.astype(bf16)
+                send_near[d, 1, piece_rows(p), :] = (c * weight).astype(bf16)
+
+            for i in range(per):
+                for d in range(2):
+                    dispatch_near(p * per + i, d).start()
+
+            return carry
+
+        lax.fori_loop(through, pieces, one, 0)
+
+    def near_ready(d, p):
+        came = rows.at[nb_tp[d], :, piece_rows(p), :]
+        remote(came, came, nb_s, nb_r.at[d, p], partner).wait_recv()
+
     give_w = [
         remote(w, part_w.at[k], misc_s.at[k], misc_r.at[k], partner)
         for k, w in enumerate((gate, up))
@@ -285,7 +348,7 @@
 
     last = (half - 1) * pieces
 
-    def ring(n_pieces, where, sems_s, sems_r, sems_ds, sems_dr, own_ready, compute, beside, stop, leap):
+    def ring(n_pieces, where, sems_s, sems_r, sems_ds, sems_dr, own_ready, compute, beside, stop, leap, side):
         h_p = n_pieces // 2
         total = (half - 1) * n_pieces + h_p
 
@@ -302,13 +365,17 @@
             if leap:
                 along(tp, p, 0, n_pieces + p, True).start()
                 along(tp, p, 1, n_pieces + p, True).start()
-            along(tp, p, 0, p).start()
-            along(tp, p, 1, p).start()
+            @pl.when((p < through) if side else (p >= 0))
+            def _():
+                along(tp, p, 0, p).start()
+                along(tp, p, 1, p).start()
+
             across(tp, p, p).start()
             return carry
 
-        lax.fori_loop(0, n_pieces, own, 0)
+        lax.fori_loop(0, 1, own, 0)
         beside()
+        lax.fori_loop(1, n_pieces, own, 0)
 
         def own_compute(p, carry):
             across(tp, p, p).wait_recv()
@@ -324,10 +391,25 @@
             hop = t // n_pieces
             return hop, p_up, p_dn
 
+        def arrive(t, d, block, p):
+            if side is None:
+                along(block, p, d, t).wait_recv()
+                return
+
+            beyond = (t >= through) & (t < n_pieces)
+
+            @pl.when(jnp.logical_not(beyond))
+            def _():
+                along(block, p, d, t).wait_recv()
+
+            @pl.when(beyond)
+            def _():
+                side(d, p)
+
         def move(t):
             hop, p_up, p_dn = at(t)
             b_up, b_dn = zpos(-1 - hop), zpos(1 + hop)
-            along(2 * b_up + core, p_up, 0, t).wait_recv()
+            arrive(t, 0, 2 * b_up + core, p_up)
             pass_up = (hop < half - 2) | ((hop == half - 2) & (p_up < h_p))
 
             @pl.when((hop == 1) if leap else pass_up)
@@ -340,7 +422,7 @@
                     along(2 * b_up + core, p_up, 0, t + 2 * n_pieces, True).start()
 
             across(2 * b_up + core, p_up, n_pieces + 2 * t).start()
-            along(2 * b_dn + core, p_dn, 1, t).wait_recv()
+            arrive(t, 1, 2 * b_dn + core, p_dn)
 
             @pl.when((hop == 1) if leap else (hop < half - 2))
             def _():
@@ -358,6 +440,13 @@
             across(2 * b_dn + core, p_dn, n_pieces + 2 * t + 1).start()
 
         def turn(u):
+            if side:
+                full = half - 1
+                v = u - full * through
+                rest = n_pieces - through
+                ringed = (u // through) * n_pieces + lax.rem(u, through)
+                sided = (v // rest) * n_pieces + through + lax.rem(jnp.maximum(v, 0), rest)
+                return jnp.where(v < 0, ringed, jnp.where(u < full * n_pieces, sided, u))
             if not leap:
                 return u
             return jnp.where(u < n_pieces, u + n_pieces, jnp.where(u < 2 * n_pieces, u - n_pieces, u))
@@ -383,9 +472,6 @@
         use(total - stop - 1)
         return move, use
 
-
-    def piece_rows(p):
-        return pl.ds(pl.multiple_of(p * chunk, chunk), chunk)
 
     def rows_ready(p):
         @pl.when((p == 0) & (per > 1))
@@ -469,6 +555,7 @@
         pre[at, 256:384] += dot_nt(c, down[:, feats(b)])
 
     early = 1 if pieces == 4 else 0
+    attend()
     move, use = ring(
         pieces,
         lambda block, p: rows.at[block, :, piece_rows(p), :],
@@ -478,9 +565,10 @@
         agd_r,
         rows_ready,
         expert_in,
-        attend,
+        near_rows,
         early,
         False,
+        near_ready,
     )
 
     h_p = pieces // 2
@@ -677,6 +765,7 @@
         lambda: None,
         0,
         half == 4,
+        None,
     )
 
     cot = mixer_cot[...]
@@ -745,7 +834,9 @@
         (ret.at[cap:, :], back_s),
         (span_in.at[1:], fw_s),
         (pj_in.at[1:], pj_s),
-        (rows.at[: n_z - 1], ag_s),
+        (near, tok_s),
+        (send_near.at[:, :, through * chunk :, :], nb_s),
+        (rows.at[: 4 * (rs_total - pieces + through) // pieces, 0], ag_s),
         (rows.at[:n_z], agd_s),
         (full_cot.at[: n_z - 1], tk_s),
         (full_cot.at[:n_z], tkd_s),
@@ -842,6 +933,8 @@
             pltpu.VMEM((n_tp, DV, cols), bf16),
             pltpu.VMEM((n_sp, wide, DV, cols), bf16),
             pltpu.VMEM((2, n_rows, cols), bf16),
+            pltpu.VMEM((2, 2, toks, cols), bf16),
+            pltpu.VMEM((2, 2, n_rows, cols), bf16),
             pltpu.VMEM((toks, n_rows), bf16),
             pltpu.VMEM((n_tp, 2, n_rows, cols), bf16),
             pltpu.VMEM((n_rows, 384), f32),
@@ -872,6 +965,10 @@
             dma((2,)),
             dma(()),
             dma((pieces,)),
+            dma(()),
+            dma((2,)),
+            dma(()),
+            dma((2, pieces)),
             dma(()),
             dma(()),
             dma((n_sp,)),

time: 130 us -> 130 us (level)
  no operation moved by 1% of the time
where the time goes in v6:
time: 130 us; the launch traced here: 127 us
  Pallas kernels  127 us (98%)
    pallas_call x1, Pallas kernels, local(): pl.pallas_call(functools.partial(moe_kernel, (n_sp, n_x, n_z, pieces)), o...  124 us
    pallas_call x1, Pallas kernels, local(): pl.pallas_call(store_kernel, out_shape=tuple((jax.ShapeDtypeStruct(g.shap...  3.18 us

profile of v6, /device:TPU:96, one launch (start us, length us, event | category | flops | bytes accessed | tf_op | source)
XLA Modules:
  0.0 127.4 jit_solution(7044205438704191239)
XLA Ops:
  0.6 123.5 %shard_map.188 = (f32[128,2048]{1,0:T(8,128)}, f32[128,2048]{1,0:T(8,128)}, f32[128,2048]{1,0:T(8,128)}, f32[128,128]{1,0:T(8,128)}, f32[64,320]{1,0:T(8,128)}, ...) custom-call(s32[2,320]{1,0:T(2,128)} %bitcast.20, f32[2,320]{1,0:T(2,128)} %bitcast.21, f32[320]{0:T(512)} %group.1, ...), custom_call_target="tpu_custom_call" | custom-call | tf_op jit(solution)/shard_map/pallas_call | solution.py:902
  124.2 3.2 %shard_map.189 = (f32[128,2048]{1,0:T(8,128)}, f32[128,2048]{1,0:T(8,128)}, f32[128,2048]{1,0:T(8,128)}, f32[128,128]{1,0:T(8,128)}, f32[64,320]{1,0:T(8,128)}, ...) custom-call(f32[128,2048]{1,0:T(8,128)} %get-tuple-element.24.refs_0_, ...), custom_call_target="tpu_custom_call" | custom-call | tf_op jit(solution)/shard_map/pallas_call | solution.py:999
